TPU v7x, 512 devices: a whole 4x4x16 slice. The times are simulated.
512 devices in a mesh: sp: 64 (over z, y), tp: 8 (over x, core).
Axes of the slice: x: 4, y: 4, z: 16, core: 2. Of those that a mesh axis runs over, the one named last changes fastest.
Arguments:
- queries: bfloat16 [16384, 1024], P('sp', 'tp'), may hold values from -6 to 6
- keys: bfloat16 [16384, 512], P('sp', 'tp'), may hold values from -6 to 6
- values: bfloat16 [16384, 512], P('sp', 'tp'), may hold values from -6 to 6
- q_gain: float32 [64], replicated, may hold values from 1.6 to 4.5
- key_norm_gain: float32 [64], replicated, may hold values from 1.6 to 4.5
- out_weight: bfloat16 [1024, 2048], P('tp'), may hold values from -0.1875 to 0.1875
- residual: bfloat16 [16384, 2048], P('sp'), may hold values from -6 to 6
- ln1_gain: float32 [2048], replicated, may hold values from 0.1 to 1.9
- ln1_bias: float32 [2048], replicated, may hold values from -3 to 3
- up_weight: bfloat16 [2048, 8192], P('sp', 'tp'), may hold values from -0.125 to 0.125
- down_weight: bfloat16 [8192, 2048], P('tp', 'sp'), may hold values from -0.0625 to 0.0625
- ln2_gain: float32 [2048], replicated, may hold values from 0.1 to 1.9
- ln2_bias: float32 [2048], replicated, may hold values from -3 to 3
Outputs:
- encoded: bfloat16 [16384, 2048], P('sp', 'tp')
All inputs are finite; a program needn't handle non-finite values.
Results may differ from a plain program's by a relative error of at most 0.014.
Values may be sent and summed in bfloat16 or wider, within the bound.
A program may use at most 64 MiB of HBM per device.

v0:
```python
import math

import jax
import jax.numpy as jnp
from jax import lax
from jax.sharding import PartitionSpec as P

D = 2048
HEAD_SIZE = 64
GRID_W = 64


ALPHA = 8.0**0.25
ROTARY_BASE = 10000.0
RMS_EPSILON = 1e-06
NORM_EPSILON = 1e-05


def turned_gather(arrays, axis, dims):
    turned = [jnp.moveaxis(a, dim, 0) for a, dim in zip(arrays, dims)]
    both = jnp.concatenate([t.reshape(len(t), -1) for t in turned], axis=1)
    out, at, finished = (lax.all_gather(both, axis, axis=0, tiled=True), 0, [])
    for t, dim in zip(turned, dims):
        piece = out[:, at : at + t[0].size].reshape(-1, *t.shape[1:])
        finished.append(jnp.moveaxis(piece, 0, dim))
        at += t[0].size
    return tuple(finished)


def side_by_side(arrays, axis, dim, along):
    widths = [a.shape[along] for a in arrays]
    both = jnp.concatenate(arrays, axis=along)
    out = lax.all_gather(both, axis, axis=dim, tiled=True)
    return tuple(jnp.split(out, [sum(widths[:k]) for k in range(1, len(widths))], axis=along))


def split_up(array, dim, devices):
    before, after = (array.shape[:dim], array.shape[dim + 1 :])
    return jnp.moveaxis(array.reshape(*before, devices, -1, *after), dim, 0)


def sent_and_summed(array, axis, dim):
    devices = lax.axis_size(axis)
    blocks = lax.all_to_all(split_up(array, dim, devices), axis, 0, 0, tiled=True)
    return jnp.sum(blocks.astype(jnp.float32), axis=0)


def from_everyone(array, axis):
    devices = lax.axis_size(axis)
    return lax.all_to_all(
        jnp.broadcast_to(array[None], (devices, *array.shape)), axis, 0, 0, tiled=True
    )


def over_copies(array, axis):
    everything = from_everyone(array, axis)
    return jnp.sum(everything, axis=0)


def in_one(arrays, axis):
    ends = [0]
    for a in arrays:
        ends.append(ends[-1] + a.size)
    running = over_copies(jnp.concatenate([a.ravel() for a in arrays]), axis)
    return tuple((running[b:e].reshape(a.shape) for a, b, e in zip(arrays, ends, ends[1:])))


def laid_out(blocks, dim):
    lengths = list(blocks.shape[1:])
    lengths[dim] *= blocks.shape[0]
    return jnp.moveaxis(blocks, 0, dim).reshape(lengths)


def gathered_copies(array, axis, dim):
    return laid_out(from_everyone(array, axis), dim)


def rotate_grid(heads_in, grid_places):
    half_dim = heads_in.shape[-1] // 2
    quarter = half_dim // 2
    inverse = ROTARY_BASE ** (-jnp.arange(quarter, dtype=jnp.float32) / quarter)

    def spin(segment, coords):
        angles = coords.astype(jnp.float32)[:, None] * inverse[None, :]
        cos_val = jnp.cos(angles)[:, None, :]
        sin_val = jnp.sin(angles)[:, None, :]
        lead_half = segment[..., :quarter]
        tail_half = segment[..., quarter:]
        return jnp.concatenate(
            [lead_half * cos_val - tail_half * sin_val, tail_half * cos_val + lead_half * sin_val],
            -1,
        )

    return jnp.concatenate(
        [
            spin(heads_in[..., :half_dim], grid_places // GRID_W),
            spin(heads_in[..., half_dim:], grid_places % GRID_W),
        ],
        -1,
    )


def prepare_inputs(heads_in, gain_vec, grid_places, factor):
    values32 = heads_in.astype(jnp.float32)
    normed = (
        values32
        * lax.rsqrt(jnp.mean(values32 * values32, -1, keepdims=True) + RMS_EPSILON)
        * gain_vec
    )
    return (rotate_grid(normed, grid_places) * factor).astype(jnp.bfloat16)


def finish_norm(pre_norm, stats, gain_vec, bias_vec):
    row_mean = stats[0][:, None] / D
    spread = stats[1][:, None] / D - row_mean * row_mean
    return (pre_norm - row_mean) * lax.rsqrt(spread + NORM_EPSILON) * gain_vec + bias_vec


def take_cols(array_in, col_start, col_width):
    return lax.dynamic_slice_in_dim(array_in, col_start, col_width, array_in.ndim - 1)


def local(
    queries,
    keys,
    values,
    q_gain,
    key_norm_gain,
    out_weight,
    residual,
    ln1_gain,
    ln1_bias,
    up_weight,
    down_weight,
    ln2_gain,
    ln2_bias,
):
    tok_rows = queries.shape[0]
    up_whole, down_whole = turned_gather((up_weight, down_weight), "sp", (0, 1))
    grid_places = lax.axis_index("sp") * tok_rows + jnp.arange(tok_rows, dtype=jnp.int32)
    kv_heads = keys.shape[1] // HEAD_SIZE
    q_count = queries.shape[1] // HEAD_SIZE
    group_count_size = q_count // kv_heads
    query_head_rows = prepare_inputs(
        queries.reshape(tok_rows, q_count, HEAD_SIZE), q_gain, grid_places, HEAD_SIZE ** (-0.5)
    )
    q_grouped = query_head_rows.reshape(tok_rows, kv_heads, group_count_size, HEAD_SIZE)
    k_sent = prepare_inputs(
        keys.reshape(tok_rows, kv_heads, HEAD_SIZE), key_norm_gain, grid_places, 1.0
    ).reshape(tok_rows, kv_heads * HEAD_SIZE)
    initial = (
        jnp.full((kv_heads, group_count_size, tok_rows), -jnp.inf, jnp.float32),
        jnp.zeros((kv_heads, group_count_size, tok_rows), jnp.float32),
        jnp.zeros((tok_rows, kv_heads, group_count_size, HEAD_SIZE), jnp.float32),
    )
    key_piece, value_piece = side_by_side((k_sent, values), "sp", 0, 1)
    key_count = key_piece.shape[0]
    block_len = math.gcd(key_count, 2048)
    key_blocks = key_piece.reshape(key_count // block_len, block_len, kv_heads, HEAD_SIZE)
    value_blocks = value_piece.reshape(key_count // block_len, block_len, kv_heads, HEAD_SIZE)

    def advance(state_in, blocks):
        maxima, totals, accumulated = state_in
        scores = jnp.einsum(
            "qhgd,khd->hgqk", q_grouped, blocks[0], preferred_element_type=jnp.float32
        )
        new_max = jnp.maximum(maxima, jnp.max(scores, -1))
        factor = jnp.exp(maxima - new_max)
        weights = jnp.exp(scores - new_max[..., None])
        totals = totals * factor + jnp.sum(weights, -1)
        update = jnp.einsum(
            "hgqk,khd->qhgd",
            weights.astype(jnp.bfloat16),
            blocks[1],
            preferred_element_type=jnp.float32,
        )
        accumulated = accumulated * jnp.transpose(factor, (2, 0, 1))[..., None] + update
        return ((new_max, totals, accumulated), None)

    state_out, unused = lax.scan(advance, initial, (key_blocks, value_blocks))
    maxima, totals, accumulated = state_out
    attended = (
        (accumulated / jnp.transpose(totals, (2, 0, 1))[..., None])
        .reshape(tok_rows, q_count * HEAD_SIZE)
        .astype(jnp.bfloat16)
    )
    partial_value = jnp.dot(attended, out_weight, preferred_element_type=jnp.float32)
    col_width = D // lax.axis_size("tp")
    col_start = lax.axis_index("tp") * col_width
    mixed_cols = sent_and_summed(partial_value.astype(jnp.bfloat16), "tp", 1)
    pre_norm = ALPHA * take_cols(residual, col_start, col_width).astype(jnp.float32) + mixed_cols
    stats = in_one((jnp.sum(pre_norm, -1), jnp.sum(pre_norm * pre_norm, -1)), "tp")
    normed_own = finish_norm(
        pre_norm,
        stats,
        take_cols(ln1_gain, col_start, col_width),
        take_cols(ln1_bias, col_start, col_width),
    ).astype(jnp.bfloat16)
    full_rows = gathered_copies(normed_own, "tp", 1)
    up_acts = jnp.dot(full_rows, up_whole, preferred_element_type=jnp.float32)
    hidden = jnp.square(jnp.maximum(up_acts, 0.0)).astype(jnp.bfloat16)
    partial_ffn = jnp.dot(hidden, down_whole, preferred_element_type=jnp.float32)
    ffn_cols = sent_and_summed(partial_ffn.astype(jnp.bfloat16), "tp", 1)
    second = ALPHA * normed_own.astype(jnp.float32) + ffn_cols
    stats_two = in_one((jnp.sum(second, -1), jnp.sum(second * second, -1)), "tp")
    return finish_norm(
        second,
        stats_two,
        take_cols(ln2_gain, col_start, col_width),
        take_cols(ln2_bias, col_start, col_width),
    ).astype(jnp.bfloat16)


def solution(mesh):
    return jax.shard_map(
        local,
        mesh=mesh,
        in_specs=(
            P("sp", "tp"),
            P("sp", "tp"),
            P("sp", "tp"),
            P(),
            P(),
            P("tp", None),
            P("sp", None),
            P(),
            P(),
            P("sp", "tp"),
            P("tp", "sp"),
            P(),
            P(),
        ),
        out_specs=P("sp", "tp"),
        check_vma=False,
    )
```

profile of v0, /device:TPU:1, one launch (start us, length us, event | category | flops | bytes accessed | tf_op | source)
XLA Modules:
  0.0 357.5 jit_solution(9664578682468562471)
XLA Ops:
  6.6 0.8 fusion.43
  7.4 0.8 fusion.45
  8.8 0.8 constant_dynamic-update-slice_fusion
  9.6 0.6 copy-done.2
  10.3 1.5 pad_maximum_fusion
  12.1 0.9 copy.36
  13.1 0.7 multiply_multiply_fusion
  13.9 137.4 %all-gather.3.cloned.1.call-done = bf16[16384,128]{0,1:T(8,128)(2,1)} async-done(((bf16[256,128]{0,1:T(8,128)(2,1)}), bf16[16384,128]{0,1:T(8,128)(2,1)}) %all-gather.3.cloned.1.call-update) | async-done | bytes 4194320 | tf_op jit(solution)/shard_map/all_gather | solution.py:33
  151.3 2.6 fusion.67
  153.9 1.2 copy.53
  155.1 1.2 copy.37
  156.2 1.2 copy.54
  157.4 2.5 copy.38
  159.9 54.9 %while.15 = (s32[]{:T(128)}, f32[1,2,256]{2,1,0:T(2,128)S(1)}, f32[1,2,256]{2,1,0:T(2,128)S(1)}, f32[256,1,2,64]{0,3,2,1:T(8,128)S(1)}, bf16[8,2048,1,64]{1,3,2,...) while((s32[]{:T(128)}, f32[1,2,256]{2,1,0:T(2,128)S(1)}, ...), condition=%wide.region_5.6_spmd.clone, body=%wide.region_2.5_spmd.clone.sunk | while | flops 273779712 | bytes 30245512 | solution.py:180
  159.9 2.7 bitcast_reduce_fusion.2
  162.7 3.2 fusion.80
  166.8 2.7 bitcast_reduce_fusion.2
  169.5 3.2 fusion.80
  173.6 2.7 bitcast_reduce_fusion.2
  176.4 3.2 fusion.80
  180.5 2.7 bitcast_reduce_fusion.2
  183.2 3.2 fusion.80
  187.4 2.7 bitcast_reduce_fusion.2
  190.1 3.2 fusion.80
  194.2 2.7 bitcast_reduce_fusion.2
  197.0 3.2 fusion.80
  201.1 2.7 bitcast_reduce_fusion.2
  203.9 3.2 fusion.80
  208.0 2.7 bitcast_reduce_fusion.2
  210.7 3.2 fusion.80
  215.4 1.1 copy.58
  216.5 14.5 %all-to-all-start = ((bf16[8,256,256]{2,1,0:T(8,128)(2,1)}), bf16[8,256,256]{2,1,0:T(8,128)(2,1)S(1)}, u32[]{:S(2)}, u32[]{:S(2)}) async-start(bf16[8,256,256]{2,1,0:T(8,128)(2,1)} %bitcast.113), calls=%async_computation | async-start | bytes 2097152 | tf_op jit(solution)/shard_map/all_to_all | solution.py:44
  231.0 15.0 %all-to-all-done = bf16[8,256,256]{2,1,0:T(8,128)(2,1)S(1)} async-done(((bf16[8,256,256]{2,1,0:T(8,128)(2,1)}), bf16[8,256,256]{2,1,0:T(8,128)(2,1)S(1)}, u32[]{:S(2)}, u32[]{:S(2)}) %all-to-all-start) | async-done | bytes 1048608 | tf_op jit(solution)/shard_map/all_to_all | solution.py:44
  246.1 1.1 fusion.46
  247.8 4.2 %all-to-all-start.1 = ((f32[8,1,512]{2,1,0:T(1,128)}), f32[8,1,512]{2,1,0:T(1,128)S(1)}, u32[]{:S(2)}, u32[]{:S(2)}) async-start(f32[8,1,512]{2,1,0:T(1,128)} %broadcast_in_dim.15), calls=%async_computation.1 | async-start | bytes 32768 | tf_op jit(solution)/shard_map/all_to_all | solution.py:50
  252.0 0.8 dynamic_slice.23
  252.7 0.8 dynamic_slice.24
  253.5 3.2 all-to-all-done.1
  256.8 1.1 add_convert_fusion.1
  258.0 18.0 %all_to_all.27 = bf16[8,256,256]{1,2,0:T(8,128)(2,1)S(1)} all-to-all(bf16[8,256,256]{1,2,0:T(8,128)(2,1)S(1)} %broadcast_in_dim.16), channel_id=1, replica_groups=mesh['sp'=64,'tp'=8] {'tp'}, dimensions={0} | all-to-all | bytes 2097152 | tf_op jit(solution)/shard_map/all_to_all | solution.py:50
  276.1 30.5 %all-gather.5.cloned.1.call-done = bf16[2048,2048]{1,0:T(8,128)(2,1)} async-done(((bf16[32,2048]{1,0:T(8,128)(2,1)}), bf16[2048,2048]{1,0:T(8,128)(2,1)}) %all-gather.5.cloned.1.call-update) | async-done | bytes 8388624 | tf_op jit(solution)/shard_map/all_gather | solution.py:22
  306.6 5.8 %fusion.26 = bf16[256,2048]{1,0:T(8,128)(2,1)S(1)} fusion(bf16[2048,2048]{1,0:T(8,128)(2,1)} %all-gather.5.cloned.1.call-done, bf16[256,2048]{0,1:T(8,128)(2,1)S(1)} %bitcast.144), kind=kOutput, calls=%fused_computation.30 | convolution fusion | flops 2148794368 | bytes 10485760 | tf_op jit(solution)/shard_map/dot_general | solution.py:202
  312.5 27.4 %all_to_all.28 = bf16[8,256,256]{2,1,0:T(8,128)(2,1)S(1)} all-to-all(bf16[8,256,256]{2,1,0:T(8,128)(2,1)S(1)} %bitcast.141), channel_id=1, replica_groups=mesh['sp'=64,'tp'=8] {'tp'}, dimensions={0} | all-to-all | bytes 2097152 | tf_op jit(solution)/shard_map/all_to_all | solution.py:44
  340.9 4.3 %all-to-all-start.4 = ((f32[8,1,512]{2,1,0:T(1,128)}), f32[8,1,512]{2,1,0:T(1,128)S(1)}, u32[]{:S(2)}, u32[]{:S(2)}) async-start(f32[8,1,512]{2,1,0:T(1,128)} %broadcast_in_dim.17), calls=%async_computation.4 | async-start | bytes 32768 | tf_op jit(solution)/shard_map/all_to_all | solution.py:50
  345.1 0.8 dynamic_slice.25
  345.9 0.8 dynamic_slice.26
  346.7 3.2 all-to-all-done.4
  349.9 0.8 add_convert_fusion
  (86 shorter events, 10.6 us)
Async XLA Ops:
  6.5 208.4 %copy-start = (bf16[128,2048]{1,0:T(8,128)(2,1)S(1)}, bf16[128,2048]{1,0:T(8,128)(2,1)}, u32[]{:S(2)}) copy-start(bf16[128,2048]{1,0:T(8,128)(2,1)} %param.20) | copy-start | bytes 1572868
  6.5 144.7 %all-gather.3.cloned.1.call-start = ((), (), s32[]{:S(2)}) async-start(), calls=%async_computation.5 | async-start | bytes 4259840 | tf_op jit(solution)/shard_map/all_gather | solution.py:33
  9.6 0.6 copy-start.2
  10.2 296.4 %all-gather.5.cloned.1.call-start = ((), (), s32[]{:S(2)}) async-start(), calls=%async_computation.6 | async-start | bytes 8519680 | tf_op jit(solution)/shard_map/all_gather | solution.py:22
  162.6 3.5 copy-start.1
  169.5 3.5 copy-start.1
  176.4 3.5 copy-start.1
  183.2 3.6 copy-start.1
  190.1 3.5 copy-start.1
  197.0 3.6 copy-start.1
  203.8 3.5 copy-start.1
  210.7 3.6 copy-start.1
  216.5 29.5 %all-to-all-start = ((bf16[8,256,256]{2,1,0:T(8,128)(2,1)}), bf16[8,256,256]{2,1,0:T(8,128)(2,1)S(1)}, u32[]{:S(2)}, u32[]{:S(2)}) async-start(bf16[8,256,256]{2,1,0:T(8,128)(2,1)} %bitcast.113), calls=%async_computation | async-start | bytes 2097152 | tf_op jit(solution)/shard_map/all_to_all | solution.py:44
  247.8 8.9 %all-to-all-start.1 = ((f32[8,1,512]{2,1,0:T(1,128)}), f32[8,1,512]{2,1,0:T(1,128)S(1)}, u32[]{:S(2)}, u32[]{:S(2)}) async-start(f32[8,1,512]{2,1,0:T(1,128)} %broadcast_in_dim.15), calls=%async_computation.1 | async-start | bytes 32768 | tf_op jit(solution)/shard_map/all_to_all | solution.py:50
  340.9 9.0 %all-to-all-start.4 = ((f32[8,1,512]{2,1,0:T(1,128)}), f32[8,1,512]{2,1,0:T(1,128)S(1)}, u32[]{:S(2)}, u32[]{:S(2)}) async-start(f32[8,1,512]{2,1,0:T(1,128)} %broadcast_in_dim.17), calls=%async_computation.4 | async-start | bytes 32768 | tf_op jit(solution)/shard_map/all_to_all | solution.py:50
Sparse Core Ops, SparseCore 0:
  10.4 140.8 all-gather.2
  154.2 152.3 all-gather.4
where the time goes:
time: 358 us; the launch traced here: 357 us
  waiting for transfers between devices  189 us (53%)
  matrix products  53.7 us (15%)
  blocking collectives  45.5 us (13%)
  starting transfers between devices  23 us (6%)
  local copies, waits for them, and re-layouts  19.1 us (5%)
  between operations  13.6 us (4%)
  other arithmetic  13 us (4%)
    all_gather x1, waiting for transfers between devices, side_by_side(): out = lax.all_gather(both, axis, axis=dim, tiled=True)  137 us
    all_gather x1, waiting for transfers between devices, turned_gather(): out, at, finished = (lax.all_gather(both, axis, axis=0, tiled=True), 0, [])  30.5 us
    all_to_all x1, blocking collectives, sent_and_summed(): lax.all_to_all(split_up(array, dim, devices), axis, 0, 0, tiled=True)  27.4 us
    dot_general x8, matrix products, advance(): jnp.einsum('hgqk,khd->qhgd', weights.astype(jnp.bfloat16), blocks[1], pre...  25.7 us
    dot_general x8, matrix products, advance(): jnp.einsum('qhgd,khd->hgqk', q_grouped, blocks[0], preferred_element_type...  21.7 us
    all_to_all x1, blocking collectives, from_everyone(): lax.all_to_all(jnp.broadcast_to(array[None], (devices, *array.shape)), ax...  18 us
    all_to_all x1, waiting for transfers between devices, sent_and_summed(): lax.all_to_all(split_up(array, dim, devices), axis, 0, 0, tiled=True)  15 us
    all_to_all x1, starting transfers between devices, sent_and_summed(): lax.all_to_all(split_up(array, dim, devices), axis, 0, 0, tiled=True)  14.5 us
  transfers between devices with their start and end apart: 5, of which 5 were waited for; matrix products, arithmetic and copies ran while one was open for 20% of the time, Pallas kernels for 0%

commit v1 on v0

v1 whole, which is shorter than its diff:
```python
import functools

import jax
import jax.numpy as jnp
import numpy as np
from jax import lax
from jax.experimental import pallas as pl
from jax.experimental.pallas import tpu as pltpu
from jax.sharding import PartitionSpec as P

HEAD = 64
GRID_W = 64
NY = 4
ALPHA = 8.0**0.25
ROTARY_BASE = 10000.0
RMS_EPSILON = 1e-06
NORM_EPSILON = 1e-05
LOG2E = 1.4426950408889634
ROWS = 256

f32, bf16 = jnp.float32, jnp.bfloat16


def rotary_tables(tokens):
    lane = np.arange(2 * HEAD) % HEAD
    pos = lane % 32
    freq = ROTARY_BASE ** (-(pos % 16) / 16.0)

    def table(count, mine):
        angle = np.arange(count)[:, None] * freq[None, :]
        cos, sin = np.cos(angle) * mine, np.sin(angle) * mine
        return np.concatenate([cos, np.where(pos < 16, -sin, 0.0), np.where(pos >= 16, sin, 0.0)], 1).astype(np.float32)

    return table(tokens // GRID_W, lane < 32), table(GRID_W, lane >= 32)


def dot(a, b, dims=((1,), (0,))):
    return lax.dot_general(a, b, (dims, ((), ())), preferred_element_type=f32)


NT = ((1,), (1,))


def kernel(
    NZ, NX, FA,
    q_ref, kv_ref, gq_ref, gk_ref, row_ref, col_ref, w_ref, wo_own, res_ref, g1_ref, b1_ref, g2_ref, b2_ref,
    out_ref,
    qb, kvb, qx, acc, mx, wb, wo, oms, omr, att, yb, res, xg, hid, part, prb, comb, rr, enc,
    q_s, q_r, kv_s, kv_r, wa_s, wa_r, wz_s, wz_r, ya_s, ya_r, yb_s, yb_r, wo_s, wo_r, wp_s, o_s, o_r, x_s, x_r, xp_s,
    p_s, p_r, r_s, r_r, e_s, e_r, loc,
):
    TP = 2 * NX
    HALF = NZ // 2
    sp, tp = lax.axis_index("sp"), lax.axis_index("tp")
    z, y = sp // NY, sp % NY
    x, core = tp // 2, tp % 2
    zr, zl = lax.rem(z + 1, NZ), lax.rem(z + NZ - 1, NZ)
    right, left = {"sp": zr * NY + y}, {"sp": zl * NY + y}
    partner = {"tp": x * 2 + 1 - core}
    me = y * TP + tp
    tok = q_ref.shape[0]
    own_rows = tok // TP
    D = wo.shape[2]

    def rc(src, dst, ss, rs, dev):
        return pltpu.make_async_remote_copy(
            src_ref=src, dst_ref=dst, send_sem=ss, recv_sem=rs, device_id=dev, device_id_type=pl.DeviceIdType.MESH
        )

    def got(ref, rs):
        rc(ref, ref, rs, rs, right).wait_recv()

    def sent(ref, ss):
        rc(ref, ref, ss, ss, right).wait_send()

    barrier = pltpu.get_barrier_semaphore()
    for dev in (right, left):
        pl.semaphore_signal(barrier, inc=1, device_id=dev, device_id_type=pl.DeviceIdType.MESH)

    @pl.loop(1, NY * TP)
    def _(i):
        d = lax.rem(me + i, NY * TP)
        pl.semaphore_signal(
            barrier, inc=1, device_id={"sp": z * NY + d // TP, "tp": lax.rem(d, TP)}, device_id_type=pl.DeviceIdType.MESH
        )

    res_copy = pltpu.make_async_copy(res_ref.at[pl.ds(tp * own_rows, own_rows), :], res, loc.at[0])
    res_copy.start()
    wo_copy = pltpu.make_async_copy(wo_own, wo.at[tp], loc.at[1])
    wo_copy.start()
    w_copy = pltpu.make_async_copy(w_ref, wb.at[sp], loc.at[2])
    w_copy.start()

    lane = lax.broadcasted_iota(jnp.int32, (1, 2 * HEAD), 1)
    low = lane < HEAD
    for r in range(tok // GRID_W):
        span = pl.ds(r * GRID_W, GRID_W)
        cs = [row_ref[r : r + 1, 128 * k : 128 * (k + 1)] + col_ref[:, 128 * k : 128 * (k + 1)] for k in range(3)]

        def turn(v, gain):
            sq = v * v
            s0 = jnp.sum(jnp.where(low, sq, 0.0), -1, keepdims=True)
            s1 = jnp.sum(jnp.where(low, 0.0, sq), -1, keepdims=True)
            inv = jnp.where(low, lax.rsqrt(s0 / HEAD + RMS_EPSILON), lax.rsqrt(s1 / HEAD + RMS_EPSILON))
            n = v * inv * gain
            return n * cs[0] + pltpu.roll(n, 112, 1) * cs[1] + pltpu.roll(n, 16, 1) * cs[2]

        qb[y, span, :] = turn(q_ref[span, :].astype(f32), gq_ref[...]).astype(bf16)
        kv = kv_ref[span, :].astype(f32)
        kvb[z, span, :] = jnp.where(low, turn(kv, gk_ref[...]), kv).astype(bf16)

    pl.semaphore_wait(barrier, NY * TP + 1)

    def send_kv(slot, to_right):
        if to_right:
            rc(kvb.at[slot], kvb.at[slot], kv_s.at[0, slot], kv_r.at[slot], right).start()
        else:
            rc(kvb.at[slot], kvb.at[slot], kv_s.at[1, slot], kv_r.at[slot], left).start()

    def wa_at(slot):
        return wb.at[pl.ds(slot * NY, NY), :, pl.ds(0, FA)]

    def wz_at(slot, row):
        return wb.at[slot * NY + row, :, pl.ds(FA, wb.shape[2] - FA)]

    def send_wa(slot, to_right):
        k, dev = (0, right) if to_right else (1, left)
        rc(wa_at(slot), wa_at(slot), wa_s.at[k, slot], wa_r.at[slot], dev).start()

    def send_wz(slot, to_right):
        k, dev = (0, right) if to_right else (1, left)
        rc(wz_at(slot, y), wz_at(slot, y), wz_s.at[k, slot], wz_r.at[slot], dev).start()

    def spread_wz(slot):
        for i in range(1, NY):
            t = lax.rem(y + i, NY)
            rc(wz_at(slot, y), wz_at(slot, y), yb_s.at[slot, i], yb_r.at[slot, y], {"sp": z * NY + t}).start()

    send_kv(z, True)
    send_kv(z, False)
    for i in range(1, NY):
        t = lax.rem(y + i, NY)
        rc(qb.at[y], qb.at[y], q_s.at[i], q_r.at[y], {"sp": z * NY + t}).start()
    w_copy.wait()
    for i in range(1, NY):
        t = lax.rem(y + i, NY)
        own = wb.at[sp, :, pl.ds(0, FA)]
        rc(own, own, ya_s.at[i], ya_r.at[y], {"sp": z * NY + t}).start()
    send_wz(z, True)
    send_wz(z, False)
    wo_copy.wait()
    for i in range(1, NX):
        t = lax.rem(x + i, NX) * 2 + core
        rc(wo.at[tp], wo.at[tp], wo_s.at[i], wo_r.at[tp], {"tp": t}).start()
    spread_wz(z)

    def spread_q(row):
        v = qb[row].astype(f32)
        h0 = jnp.where(low, v, 0.0).astype(bf16)
        h1 = jnp.where(low, pltpu.roll(v, HEAD, 1), 0.0).astype(bf16)
        for t in range(TP):
            at = (row * TP + t) * 2 * own_rows
            part_rows = slice(t * own_rows, (t + 1) * own_rows)
            qx[pl.ds(pl.multiple_of(at, own_rows), own_rows), :] = h0[part_rows]
            qx[pl.ds(pl.multiple_of(at + own_rows, own_rows), own_rows), :] = h1[part_rows]

    def flash(slots):
        kvs = [kvb[s] for s in slots]
        ones = [jnp.where(low, jnp.ones_like(k), k) for k in kvs]

        @pl.loop(0, qx.shape[0] // ROWS)
        def _(c):
            rows = pl.ds(pl.multiple_of(c * ROWS, ROWS), ROWS)
            qv = qx[rows, :]
            ss = [dot(qv, k, NT) for k in kvs]
            top = jnp.max(functools.reduce(jnp.maximum, ss), -1, keepdims=True)
            old = mx[rows, :]
            new = jnp.maximum(old, top)
            ps = [jnp.exp2(s - new[:, :1]).astype(bf16) for s in ss]
            add = functools.reduce(jnp.add, [dot(p, v) for p, v in zip(ps, ones)])
            acc[rows, :] = acc[rows, :] * jnp.exp2(old - new) + add
            mx[rows, :] = new

    acc[...] = jnp.zeros_like(acc)
    mx[...] = jnp.full_like(mx, -1e30)
    spread_q(y)
    for i in range(1, NY):
        t = lax.rem(y + i, NY)
        got(wb.at[z * NY + t, :, pl.ds(0, FA)], ya_r.at[t])
    send_wa(z, True)
    send_wa(z, False)
    for i in range(1, NY):
        t = lax.rem(y + i, NY)
        got(qb.at[t], q_r.at[t])
        spread_q(t)
    flash([z])

    @pl.loop(1, HALF)
    def _(s):
        a, b = lax.rem(z + NZ - s, NZ), lax.rem(z + s, NZ)
        more = s < HALF - 1
        got(kvb.at[a], kv_r.at[a])
        send_kv(a, True)
        got(kvb.at[b], kv_r.at[b])

        @pl.when(more)
        def _():
            send_kv(b, False)

        got(wz_at(a, y), wz_r.at[a])
        send_wz(a, True)
        got(wz_at(b, y), wz_r.at[b])

        @pl.when(more)
        def _():
            send_wz(b, False)

        got(wa_at(a), wa_r.at[a])
        send_wa(a, True)
        got(wa_at(b), wa_r.at[b])

        @pl.when(more)
        def _():
            send_wa(b, False)

        spread_wz(a)
        spread_wz(b)
        flash([a, b])

    far = lax.rem(z + HALF, NZ)
    got(kvb.at[far], kv_r.at[far])
    flash([far])

    @pl.loop(0, NY * TP)
    def _(i):
        d = lax.rem(me + 1 + i, NY * TP)
        span = pl.ds(pl.multiple_of(d * 2 * own_rows, 2 * own_rows), 2 * own_rows)
        a = acc[span, :]
        total = a[:, :1]
        lse = mx[span, :] + jnp.log2(total)
        hi = lse.astype(bf16).astype(f32)
        mid = (lse - hi).astype(bf16).astype(f32)
        sumparts = jnp.where(lane < 16, hi, jnp.where(lane < 32, mid, jnp.where(lane < 48, lse - hi - mid, 0.0)))
        message = jnp.where(low, sumparts, a / total).astype(bf16)

        @pl.when(d == me)
        def _():
            omr[me] = message

        @pl.when(d != me)
        def _():
            oms[d] = message
            rc(oms.at[d], omr.at[me], o_s.at[d], o_r.at[me], {"sp": z * NY + d // TP, "tp": lax.rem(d, TP)}).start()

    for i in range(1, NX):
        t = lax.rem(x + i, NX) * 2 + core
        got(wo.at[t], wo_r.at[t])
    for i in range(NX):
        t = lax.rem(x + i, NX) * 2 + core
        rc(wo.at[t], wo.at[t], wp_s.at[i], wo_r.at[t], partner).start()

    got(wz_at(far, y), wz_r.at[far])
    spread_wz(far)

    @pl.loop(1, NY * TP)
    def _(i):
        d = lax.rem(me + i, NY * TP)
        got(omr.at[d], o_r.at[d])

    @pl.loop(0, TP)
    def _(t):
        msgs = [omr[r * TP + t].astype(f32) for r in range(NY)]
        lses = [jnp.sum(jnp.where(lane < 48, m, 0.0), -1, keepdims=True) * (1.0 / 16.0) for m in msgs]
        top = functools.reduce(jnp.maximum, lses)
        ws = [jnp.exp2(v - top) for v in lses]
        o = functools.reduce(jnp.add, [w * m for w, m in zip(ws, msgs)]) / functools.reduce(jnp.add, ws)
        both = jnp.where(low, pltpu.roll(o[:own_rows], HEAD, 1), o[own_rows:])
        att[:, pl.ds(pl.multiple_of(t * 128, 128), 128)] = both.astype(bf16)

    for i in range(NX):
        t = lax.rem(x + i, NX) * 2 + 1 - core
        got(wo.at[t], wo_r.at[t])
    res_copy.wait()

    CW = 256

    @pl.loop(0, D // CW)
    def _(n):
        cols = pl.ds(pl.multiple_of(n * CW, CW), CW)
        w = wo[:, :, cols].reshape(TP * 128, CW)
        yb[:, cols] = dot(att[...], w) + ALPHA * res[:, cols].astype(f32)

    def norm(v, gain, bias):
        mean = jnp.mean(v, -1, keepdims=True)
        c = v - mean
        return c * lax.rsqrt(jnp.mean(c * c, -1, keepdims=True) + NORM_EPSILON) * gain + bias

    xg[tp] = norm(yb[...], g1_ref[...], b1_ref[...]).astype(bf16)
    for i in range(1, NX):
        t = lax.rem(x + i, NX) * 2 + core
        rc(xg.at[tp], xg.at[tp], x_s.at[i], x_r.at[tp], {"tp": t}).start()
    rc(xg.at[tp], xg.at[tp], xp_s.at[0], x_r.at[tp], partner).start()
    for i in range(1, NX):
        t = lax.rem(x + i, NX) * 2 + core
        got(xg.at[t], x_r.at[t])
        rc(xg.at[t], xg.at[t], xp_s.at[i], x_r.at[t], partner).start()

    got(wa_at(far), wa_r.at[far])

    @pl.loop(0, NZ)
    def _(s):
        for i in range(1, NY):
            t = lax.rem(y + i, NY)
            got(wz_at(s, t), yb_r.at[s, t])

    for i in range(NX):
        t = lax.rem(x + i, NX) * 2 + 1 - core
        got(xg.at[t], x_r.at[t])

    FW = wb.shape[2]
    piece = w_ref.shape[0] // 2
    per = 256 // piece

    @pl.loop(0, FW // CW)
    def _(n):
        cols = pl.ds(pl.multiple_of(n * CW, CW), CW)
        up = dot(xg[...].reshape(tok, D), wb[:, :piece, cols].reshape(D, CW))
        hid[:, cols] = jnp.square(jnp.maximum(up, 0.0)).astype(bf16)

    @pl.loop(0, D // 256)
    def _(n):
        w = wb[pl.ds(n * per, per), piece:, :].reshape(256, FW)
        ffn = dot(hid[...], w, NT).astype(bf16)
        part[:, :, pl.ds(pl.multiple_of(n * 256, 256), 256)] = ffn.reshape(TP, own_rows, 256)

    for i in range(NX):
        t = lax.rem(x + i, NX)
        rc(part.at[t * 2 + 1 - core], prb.at[t], p_s.at[i], p_r.at[t], partner).start()
    for i in range(1, NX):
        t = lax.rem(x + i, NX)
        got(prb.at[t], p_r.at[t])
        comb[t] = (part[t * 2 + core].astype(f32) + prb[t].astype(f32)).astype(bf16)
        rc(comb.at[t], rr.at[x], r_s.at[i], r_r.at[x], {"tp": t * 2 + core}).start()
    got(prb.at[x], p_r.at[x])
    yb[...] = part[tp].astype(f32) + prb[x].astype(f32) + ALPHA * xg[tp].astype(f32)
    for i in range(1, NX):
        t = lax.rem(x + i, NX)
        got(rr.at[t], r_r.at[t])
        yb[...] += rr[t].astype(f32)
    last = norm(yb[...], g2_ref[...], b2_ref[...]).astype(bf16)
    wide = D // TP
    for t in range(TP):
        enc[t] = last[:, t * wide : (t + 1) * wide]
    mine = pl.ds(tp * own_rows, own_rows)
    for i in range(1, TP):
        t = lax.rem(tp + i, TP)
        rc(enc.at[t], out_ref.at[mine, :], e_s.at[i], e_r.at[tp], {"tp": t}).start()
    out_ref[mine, :] = enc[tp]
    for i in range(1, TP):
        t = lax.rem(tp + i, TP)
        got(out_ref.at[pl.ds(t * own_rows, own_rows), :], e_r.at[t])

    for i in range(1, NY):
        sent(qb.at[y], q_s.at[i])
        sent(wb.at[sp, :, pl.ds(0, FA)], ya_s.at[i])
    for i in range(1, NX):
        sent(wo.at[tp], wo_s.at[i])
        sent(xg.at[tp], x_s.at[i])
        sent(comb.at[0], r_s.at[i])
    for i in range(NX):
        sent(wo.at[tp], wp_s.at[i])
        sent(xg.at[tp], xp_s.at[i])
        sent(part.at[0], p_s.at[i])
    for i in range(1, TP):
        sent(enc.at[0], e_s.at[i])

    @pl.loop(1, NY * TP)
    def _(i):
        d = lax.rem(me + i, NY * TP)
        sent(oms.at[d], o_s.at[d])

    @pl.loop(0, NZ)
    def _(s):
        for i in range(1, NY):
            sent(wz_at(s, y), yb_s.at[s, i])

    @pl.loop(0, HALF)
    def _(s):
        a, b = lax.rem(z + NZ - s, NZ), lax.rem(z + s, NZ)
        sent(kvb.at[a], kv_s.at[0, a])
        sent(wa_at(a), wa_s.at[0, a])
        sent(wz_at(a, y), wz_s.at[0, a])

        @pl.when(s < HALF - 1)
        def _():
            sent(kvb.at[b], kv_s.at[1, b])
            sent(wa_at(b), wa_s.at[1, b])
            sent(wz_at(b, y), wz_s.at[1, b])


def solution(mesh):
    SP, TP = mesh.shape["sp"], mesh.shape["tp"]
    NZ, NX = SP // NY, TP // 2

    def local(queries, keys, values, q_gain, key_norm_gain, out_weight, residual, ln1_gain, ln1_bias, up_weight, down_weight, ln2_gain, ln2_bias):
        tok, D, FW = queries.shape[0], out_weight.shape[1], up_weight.shape[1]
        own = tok // TP
        FA = (FW // 128 * 3 // 8) * 128
        piece = up_weight.shape[0]
        rows, cols = rotary_tables(tok * SP)
        per = tok // GRID_W
        rows = lax.dynamic_slice_in_dim(jnp.asarray(rows), lax.axis_index("sp") * per, per, 0)
        kv = jnp.concatenate([keys, values], axis=1)
        w = jnp.concatenate([up_weight, down_weight.T], axis=0)
        gq = jnp.tile(q_gain * (HEAD**-0.5 * LOG2E), 2)[None, :]
        gk = jnp.concatenate([key_norm_gain, jnp.ones_like(key_norm_gain)])[None, :]
        vm, hbm = pl.BlockSpec(memory_space=pltpu.VMEM), pl.BlockSpec(memory_space=pl.ANY)
        dma = pltpu.SemaphoreType.DMA
        V = pltpu.VMEM
        flops = 2 * tok * tok * SP * 256 + 4 * tok * D * FW
        return pl.pallas_call(
            functools.partial(kernel, NZ, NX, FA),
            out_shape=jax.ShapeDtypeStruct((tok, D // TP), bf16),
            in_specs=[vm, vm, vm, vm, vm, vm, hbm, hbm, hbm, vm, vm, vm, vm],
            out_specs=vm,
            scratch_shapes=[
                V((NY, tok, 128), bf16), V((NZ, tok, 128), bf16), V((NY * tok * 2, 128), bf16),
                V((NY * tok * 2, 128), f32), V((NY * tok * 2, 128), f32),
                V((SP, 2 * piece, FW), bf16), V((TP, 128, D), bf16),
                V((NY * TP, 2 * own, 128), bf16), V((NY * TP, 2 * own, 128), bf16), V((own, TP * 128), bf16),
                V((own, D), f32), V((own, D), bf16), V((TP, own, D), bf16), V((tok, FW), bf16), V((TP, own, D), bf16),
                V((NX, own, D), bf16), V((NX, own, D), bf16), V((NX, own, D), bf16), V((TP, own, D // TP), bf16),
                dma((NY,)), dma((NY,)), dma((2, NZ)), dma((NZ,)), dma((2, NZ)), dma((NZ,)), dma((2, NZ)), dma((NZ,)),
                dma((NY,)), dma((NY,)), dma((NZ, NY)), dma((NZ, NY)), dma((NX,)), dma((TP,)), dma((NX,)),
                dma((NY * TP,)), dma((NY * TP,)), dma((NX,)), dma((TP,)), dma((NX,)),
                dma((NX,)), dma((NX,)), dma((NX,)), dma((NX,)), dma((TP,)), dma((TP,)), dma((3,)),
            ],
            compiler_params=pltpu.CompilerParams(collective_id=0, has_side_effects=True, vmem_limit_bytes=60000000),
            cost_estimate=pl.CostEstimate(flops=flops, bytes_accessed=30000000, transcendentals=0),
        )(queries, kv, gq, gk, rows, jnp.asarray(cols), w, out_weight, residual, ln1_gain[None], ln1_bias[None], ln2_gain[None], ln2_bias[None])

    return jax.shard_map(
        local,
        mesh=mesh,
        in_specs=(
            P("sp", "tp"), P("sp", "tp"), P("sp", "tp"), P(), P(), P("tp", None), P("sp", None),
            P(), P(), P("sp", "tp"), P("tp", "sp"), P(), P(),
        ),
        out_specs=P("sp", "tp"),
        check_vma=False,
    )
```

time: 358 us -> 138 us (0.39)
  waiting for transfers between devices: 189 us -> 0 us
  Pallas kernels: 0 us -> 130 us
  matrix products: 53.7 us -> 0 us
  blocking collectives: 45.5 us -> 0 us
  starting transfers between devices: 23 us -> 0 us
  between operations: 13.6 us -> 0.04 us
  local copies, waits for them, and re-layouts: 19.1 us -> 5.65 us
  other arithmetic: 13 us -> 2.04 us
    all_gather x2 -> x0, waiting for transfers between devices: 168 us -> none  [the longest x1 137 us: side_by_side(): out = lax.all_gather(both, axis, axis=dim, tiled=True)]
    pallas_call x0 -> x1, Pallas kernels: none -> 130 us  [local(): pl.pallas_call(functools.partial(kernel, NZ, NX, FA), out_shape=jax.Shape...]
    dot_general x18 -> x0, matrix products: 53.7 us -> none  [the longest x8 25.7 us: advance(): jnp.einsum('hgqk,khd->qhgd', weights.astype(jnp.bfloat16), blocks[1], pre...]
    all_to_all x2 -> x0, blocking collectives: 45.5 us -> none  [the longest x1 27.4 us: sent_and_summed(): lax.all_to_all(split_up(array, dim, devices), axis, 0, 0, tiled=True)]
    all_to_all x3 -> x0, starting transfers between devices: 23 us -> none  [the longest x1 14.5 us: sent_and_summed(): lax.all_to_all(split_up(array, dim, devices), axis, 0, 0, tiled=True)]
    all_to_all x3 -> x0, waiting for transfers between devices: 21.3 us -> none  [the longest x1 15 us: sent_and_summed(): lax.all_to_all(split_up(array, dim, devices), axis, 0, 0, tiled=True)]
    reduce_sum x16 -> x0, other arithmetic: 6.94 us -> none  [the longest x8 4.52 us: advance(): totals = totals * factor + jnp.sum(weights, -1)]
    unnamed x8 -> x11, local copies, waits for them, and re-layouts: 6.66 us -> 2.59 us
  transfers between devices with their start and end apart: 5 -> 0, of which waited for: 5 -> 0; matrix products, arithmetic and copies ran while one was open for 20% -> 0% of each run, Pallas kernels for 0% -> 0%
where the time goes in v1:
time: 138 us
  Pallas kernels  130 us (94%)
  local copies, waits for them, and re-layouts  5.65 us (4%)
  other arithmetic  2.04 us (1%)
    pallas_call x1, Pallas kernels, local(): pl.pallas_call(functools.partial(kernel, NZ, NX, FA), out_shape=jax.Shape...  130 us

profile of v1, /device:TPU:1, one launch (start us, length us, event | category | flops | bytes accessed | tf_op | source)
XLA Modules:
  0.0 137.9 jit_solution(11796878592059752567)
XLA Ops:
  0.0 0.0 copy-start.2
  0.0 0.7 broadcast_multiply_fusion
  0.7 0.6 broadcast_in_dim_tile.3.gq_ref
  1.3 1.1 pad_bitcast_fusion.gk_ref
  2.4 1.3 constant_dynamic-slice_fusion.row_ref
  3.7 0.0 copy-done.2
  3.7 0.0 copy-start.3
  3.7 0.1 copy.16
  3.8 0.6 copy-done.3
  4.5 0.1 copy.17
  4.6 0.0 copy-start
  4.6 0.0 copy-start.1
  4.6 0.7 pad_maximum_fusion.1.kv_ref
  5.3 0.1 copy-done
  5.5 0.0 copy-done.1
  5.5 0.7 pad_maximum_fusion.w_ref
  6.1 130.1 %shard_map.145 = bf16[256,256]{1,0:T(8,128)(2,1)} custom-call(bf16[256,128]{1,0:T(8,128)(2,1)} %q_ref.1, bf16[256,128]{1,0:T(8,128)(2,1)} %pad_maximum_fusion.1.kv_ref, f32[1,128]{1,0:T(1,128)} %broadcast_in_dim_tile.3.gq_ref, f32[1,128]{1,0:T(1,128)} %pad_bitcast_fusion.gk_ref, f32[4,384]{1,0:T(4,128)} %constant_dynamic-slice_fusion.row_ref, ...), custom_call_target="tpu_custom_call" | custom-call | flops 4294967296 | bytes 30000000 | tf_op jit(solution)/shard_map/pallas_call | solution.py:421
  136.3 1.6 %copy.19 = bf16[256,256]{1,0:T(8,128)(2,1)} copy(bf16[256,256]{1,0:T(8,128)(2,1)} %shard_map.145) | data formatting | bytes 262144
  (1 shorter events, 0.0 us)
Async XLA Ops:
  0.0 3.7 %copy-start.2 = (bf16[256,64]{0,1:T(8,128)(2,1)S(1)}, bf16[256,64]{0,1:T(8,128)(2,1)}, u32[]{:S(2)}) copy-start(bf16[256,64]{0,1:T(8,128)(2,1)} %param.16) | copy-start | bytes 98308
  3.7 0.8 copy-start.3
  4.6 0.8 copy-start
  4.6 0.9 copy-start.1

commit v2 on v1

v2 whole, which is shorter than its diff:
```python
import functools

import jax
import jax.numpy as jnp
import numpy as np
from jax import lax
from jax.experimental import pallas as pl
from jax.experimental.pallas import tpu as pltpu
from jax.sharding import PartitionSpec as P

HEAD = 64
GRID_W = 64
NY = 4
ALPHA = 8.0**0.25
ROTARY_BASE = 10000.0
RMS_EPSILON = 1e-06
NORM_EPSILON = 1e-05
LOG2E = 1.4426950408889634
f32, bf16 = jnp.float32, jnp.bfloat16


def rotary_tables(tokens, devices):
    lane = np.arange(2 * HEAD) % HEAD
    pos = lane % 32
    freq = ROTARY_BASE ** (-(pos % 16) / 16.0)

    def table(count, mine):
        angle = np.arange(count)[:, None] * freq[None, :]
        cos, sin = np.cos(angle) * mine, np.sin(angle) * mine
        return np.concatenate([cos, np.where(pos < 16, -sin, 0.0), np.where(pos >= 16, sin, 0.0)], 1).astype(np.float32)

    rows = table(tokens // GRID_W, lane < 32).reshape(devices, -1, 6 * HEAD)
    return np.pad(rows, ((0, 0), (0, -rows.shape[1] % 8), (0, 0))), table(GRID_W, lane >= 32)


def dot(a, b, dims=((1,), (0,))):
    return lax.dot_general(a, b, (dims, ((), ())), preferred_element_type=f32)


NT = ((1,), (1,))


def kernel(
    NZ, NX, FA,
    q_ref, k_ref, v_ref, gq_ref, gk_ref, row_ref, col_ref, up_ref, down_ref, wo_own, res_ref, g1_ref, b1_ref, g2_ref, b2_ref,
    out_ref,
    rowv, qb, kvb, qx, acc, mx, wb, wo, oms, omr, att, yb, res, xg, hid, part, prb, comb, rr, enc,
    q_s, q_r, kv_s, kv_r, wa_s, wa_r, wz_s, wz_r, ya_s, ya_r, yf_s, yf_r, yh_r, wo_s, wo_r, wp_s, o_s, o_r, x_s, x_r, xp_s,
    p_s, p_r, r_s, r_r, e_s, e_r, loc,
):
    TP = 2 * NX
    HALF = NZ // 2
    sp, tp = lax.axis_index("sp"), lax.axis_index("tp")
    z, y = sp // NY, lax.rem(sp, NY)
    x, core = tp // 2, lax.rem(tp, 2)
    zr, zl = lax.rem(z + 1, NZ), lax.rem(z + NZ - 1, NZ)
    yu, yd = lax.rem(y + 1, NY), lax.rem(y + NY - 1, NY)
    right, left = {"sp": zr * NY + y}, {"sp": zl * NY + y}
    above, below = {"sp": z * NY + yu}, {"sp": z * NY + yd}
    partner = {"tp": x * 2 + 1 - core}
    me = y * TP + tp
    tok = q_ref.shape[0]
    own_rows = tok // TP
    D = wo.shape[2]
    FW = wb.shape[2]
    piece = up_ref.shape[0]

    def rc(src, dst, ss, rs, dev):
        return pltpu.make_async_remote_copy(
            src_ref=src, dst_ref=dst, send_sem=ss, recv_sem=rs, device_id=dev, device_id_type=pl.DeviceIdType.MESH
        )

    def got(ref, rs):
        rc(ref, ref, rs, rs, right).wait_recv()

    def sent(ref, ss):
        rc(ref, ref, ss, ss, right).wait_send()

    barrier = pltpu.get_barrier_semaphore()
    for dev in (right, left):
        pl.semaphore_signal(barrier, inc=1, device_id=dev, device_id_type=pl.DeviceIdType.MESH)

    @pl.loop(1, NY * TP)
    def _(i):
        d = lax.rem(me + i, NY * TP)
        pl.semaphore_signal(
            barrier, inc=1, device_id={"sp": z * NY + d // TP, "tp": lax.rem(d, TP)}, device_id_type=pl.DeviceIdType.MESH
        )

    copies = [
        pltpu.make_async_copy(row_ref.at[sp], rowv, loc.at[0]),
        pltpu.make_async_copy(up_ref, wb.at[sp, pl.ds(0, piece), :], loc.at[1]),
        pltpu.make_async_copy(down_ref, wb.at[sp, pl.ds(piece, piece), :], loc.at[2]),
        pltpu.make_async_copy(wo_own, wo.at[tp], loc.at[3]),
        pltpu.make_async_copy(res_ref.at[pl.ds(tp * own_rows, own_rows), :], res, loc.at[4]),
    ]
    for c in copies:
        c.start()

    lane = lax.broadcasted_iota(jnp.int32, (1, 2 * HEAD), 1)
    low = lane < HEAD
    kv_all = jnp.transpose(jnp.concatenate([k_ref[...].astype(f32), v_ref[...].astype(f32)], 0))
    gq = jnp.concatenate([gq_ref[...], gq_ref[...]], 1) * (HEAD**-0.5 * LOG2E)
    gk = jnp.concatenate([gk_ref[...], gk_ref[...]], 1)
    copies[0].wait()

    def spans():
        for r in range(tok // GRID_W):
            cs = [rowv[r : r + 1, 128 * k : 128 * (k + 1)] + col_ref[:, 128 * k : 128 * (k + 1)] for k in range(3)]
            yield pl.ds(r * GRID_W, GRID_W), cs, kv_all[r * GRID_W : (r + 1) * GRID_W]

    def turn(v, gain, cs):
        sq = v * v
        s0 = jnp.sum(jnp.where(low, sq, 0.0), -1, keepdims=True)
        s1 = jnp.sum(jnp.where(low, 0.0, sq), -1, keepdims=True)
        inv = jnp.where(low, lax.rsqrt(s0 / HEAD + RMS_EPSILON), lax.rsqrt(s1 / HEAD + RMS_EPSILON))
        n = v * inv * gain
        return n * cs[0] + pltpu.roll(n, 112, 1) * cs[1] + pltpu.roll(n, 16, 1) * cs[2]

    for span, cs, kv in spans():
        kvb[z, span, :] = jnp.where(low, turn(kv, gk, cs), kv).astype(bf16)

    pl.semaphore_wait(barrier, NY * TP + 1)

    def wa_at(slot, k):
        return wb.at[pl.ds(slot * NY + k * (NY // 2), NY // 2), :, pl.ds(0, FA)]

    def wz_at(slot, row):
        return wb.at[slot * NY + row, :, pl.ds(FA, FW - FA)]

    def half_at(slot, row, k):
        return wb.at[slot * NY + row, pl.ds(k * piece, piece), pl.ds(FA, FW - FA)]

    def send_kv(slot, dev):
        rc(kvb.at[slot], kvb.at[slot], kv_s, kv_r.at[slot], dev).start()

    def send_wa(slot, dev, k):
        rc(wa_at(slot, k), wa_at(slot, k), wa_s, wa_r.at[slot, k], dev).start()

    def send_wz(slot, dev):
        rc(wz_at(slot, y), wz_at(slot, y), wz_s, wz_r.at[slot], dev).start()

    def minus(s):
        return lax.rem(z + NZ - s, NZ)

    def plus(s):
        return lax.rem(z + s, NZ)

    def both(s, ref, sem, send, send_first, send_last):
        def onward():
            send(minus(s), right)

        def last():
            send_first(minus(s), right)

        got(ref(minus(s)), sem.at[minus(s)])
        if isinstance(s, int):
            onward() if s < HALF - 1 else last()
        else:
            pl.when(s < HALF - 1)(onward)
            pl.when(s == HALF - 1)(last)
        got(ref(plus(s)), sem.at[plus(s)])
        if isinstance(s, int):
            send(plus(s), left) if s < HALF - 1 else send_last(plus(s), left)
        else:
            pl.when(s < HALF - 1)(lambda: send(plus(s), left))
            pl.when(s == HALF - 1)(lambda: send_last(plus(s), left))

    def step_kv(s):
        def part_of(lo):
            def f(i, dev):
                r = kvb.at[i, pl.ds(lo, tok // 2), :]
                rc(r, r, kv_s, kv_r.at[i], dev).start()

            return f

        both(s, lambda i: kvb.at[i], kv_r, send_kv, part_of(0), part_of(tok // 2))

    def step_wz(s):
        def part_of(k):
            def f(i, dev):
                rc(half_at(i, y, k), half_at(i, y, k), wz_s, wz_r.at[i], dev).start()

            return f

        both(s, lambda i: wz_at(i, y), wz_r, send_wz, part_of(0), part_of(1))

    def step_wa(s):
        for k in range(2):

            def nothing(i, dev):
                pass

            def go(i, dev, k=k):
                send_wa(i, dev, k)

            both(s, lambda i, k=k: wa_at(i, k), wa_r.at[:, k], go, go if k == 0 else nothing, go if k == 1 else nothing)

    def spread(slot):
        rc(wz_at(slot, y), wz_at(slot, y), yf_s, yf_r.at[slot, 0], above).start()
        rc(wz_at(slot, y), wz_at(slot, y), yf_s, yf_r.at[slot, 1], below).start()

    def relay(slot):
        got(wz_at(slot, yd), yf_r.at[slot, 0])
        rc(half_at(slot, yd, 0), half_at(slot, yd, 0), yf_s, yh_r, above).start()
        got(wz_at(slot, yu), yf_r.at[slot, 1])
        rc(half_at(slot, yu, 1), half_at(slot, yu, 1), yf_s, yh_r, below).start()

    def pair(s, f):
        f(minus(s))
        f(plus(s))

    send_kv(z, right)
    send_kv(z, left)
    copies[1].wait()
    copies[2].wait()
    for i in range(1, NY):
        t = lax.rem(y + i, NY)
        own = wb.at[sp, :, pl.ds(0, FA)]
        rc(own, own, ya_s, ya_r.at[y], {"sp": z * NY + t}).start()
    send_wz(z, right)
    send_wz(z, left)
    for span, cs, kv in spans():
        qb[y, span, :] = turn(q_ref[span, :].astype(f32), gq, cs).astype(bf16)
    for i in range(1, NY):
        t = lax.rem(y + i, NY)
        rc(qb.at[y], qb.at[y], q_s, q_r.at[y], {"sp": z * NY + t}).start()
    spread(z)
    copies[3].wait()
    for i in range(1, NX):
        t = lax.rem(x + i, NX) * 2 + core
        rc(wo.at[tp], wo.at[tp], wo_s, wo_r.at[0], {"tp": t}).start()

    def spread_q(row):
        v = qb[row].astype(f32)
        h0 = jnp.where(low, v, 0.0).astype(bf16)
        h1 = jnp.where(low, pltpu.roll(v, HEAD, 1), 0.0).astype(bf16)
        for t in range(TP):
            at = (row * TP + t) * 2 * own_rows
            part_rows = slice(t * own_rows, (t + 1) * own_rows)
            qx[pl.ds(pl.multiple_of(at, own_rows), own_rows), :] = h0[part_rows]
            qx[pl.ds(pl.multiple_of(at + own_rows, own_rows), own_rows), :] = h1[part_rows]

    def flash(slots):
        kvs = [kvb[s] for s in slots]
        ones = [jnp.where(low, jnp.ones_like(k), k) for k in kvs]
        ss = [dot(qx[...], k, NT) for k in kvs]
        top = jnp.max(functools.reduce(jnp.maximum, ss), -1, keepdims=True)
        old = mx[...]
        new = jnp.maximum(old, top)
        wide = jnp.concatenate([new] * (tok // 128), 1) if tok > 128 else new[:, :tok]
        ps = [jnp.exp2(s - wide).astype(bf16) for s in ss]
        add = functools.reduce(jnp.add, [dot(p, v) for p, v in zip(ps, ones)])
        acc[...] = acc[...] * jnp.exp2(old - new) + add
        mx[...] = new

    acc[...] = jnp.zeros_like(acc)
    mx[...] = jnp.full_like(mx, -1e30)
    spread_q(y)
    NA = (HALF - 1) // 3
    SM = HALF - 3

    @pl.loop(1, HALF)
    def _(s):
        step_kv(s)
        step_wz(s)

        @pl.when(s == 1)
        def _():
            for i in range(1, NY):
                t = lax.rem(y + i, NY)
                got(wb.at[z * NY + t, :, pl.ds(0, FA)], ya_r.at[t])
            for k in range(2):
                send_wa(z, right, k)
                send_wa(z, left, k)
            for i in range(1, NY):
                t = lax.rem(y + i, NY)
                got(qb.at[t], q_r.at[t])
                spread_q(t)
            flash([z])

        @pl.when(lax.rem(s, 3) == 0)
        def _():
            step_wa(s // 3)

        @pl.when(s <= SM)
        def _():
            pair(s, spread)

        flash([minus(s), plus(s)])

        @pl.when(s <= SM + 1)
        def _():
            relay(minus(s - 1))

            @pl.when(s > 1)
            def _():
                relay(plus(s - 1))

    far = lax.rem(z + HALF, NZ)
    got(kvb.at[far], kv_r.at[far])
    flash([far])

    total = pltpu.roll(acc[...], HEAD, 1)
    lse = mx[...] + jnp.log2(acc[...])
    hi = lse.astype(bf16).astype(f32)
    mid = (lse - hi).astype(bf16).astype(f32)
    sumparts = jnp.where(lane < 16, hi, jnp.where(lane < 32, mid, jnp.where(lane < 48, lse - hi - mid, 0.0)))
    oms[...] = jnp.where(low, sumparts, acc[...] / total).astype(bf16).reshape(oms.shape)

    @pl.loop(1, NY * TP)
    def _(i):
        d = lax.rem(me + i, NY * TP)
        rc(oms.at[d], omr.at[me], o_s, o_r, {"sp": z * NY + d // TP, "tp": lax.rem(d, TP)}).start()

    omr[me] = oms[me]
    for s in range(SM + 1, HALF):
        pair(s, spread)
    step_wa(NA + 1)
    if NX > 1:
        got(wo.at[pl.ds(0, NX - 1)], wo_r.at[0])
    for i in range(NX):
        t = lax.rem(x + i, NX) * 2 + core
        rc(wo.at[t], wo.at[t], wp_s, wo_r.at[1], partner).start()
    got(wz_at(far, y), wz_r.at[far])
    spread(far)
    mid_a = min(NA + 3, HALF - 1)
    for s in range(NA + 2, mid_a + 1):
        step_wa(s)
    got(omr.at[pl.ds(0, NY * TP - 1)], o_r)

    @pl.loop(0, TP)
    def _(t):
        msgs = [omr[r * TP + t].astype(f32) for r in range(NY)]
        lses = [jnp.sum(jnp.where(lane < 48, m, 0.0), -1, keepdims=True) * (1.0 / 16.0) for m in msgs]
        top = functools.reduce(jnp.maximum, lses)
        ws = [jnp.exp2(v - top) for v in lses]
        o = functools.reduce(jnp.add, [w * m for w, m in zip(ws, msgs)]) / functools.reduce(jnp.add, ws)
        heads = jnp.where(low, pltpu.roll(o[:own_rows], HEAD, 1), o[own_rows:])
        att[:, pl.ds(pl.multiple_of(t * 128, 128), 128)] = heads.astype(bf16)

    got(wo.at[pl.ds(0, NX)], wo_r.at[1])
    copies[4].wait()

    CW = 256

    @pl.loop(0, D // CW)
    def _(n):
        cols = pl.ds(pl.multiple_of(n * CW, CW), CW)
        w = wo[:, :, cols].reshape(TP * 128, CW)
        yb[:, cols] = dot(att[...], w) + ALPHA * res[:, cols].astype(f32)

    def norm(v, gain, bias):
        mean = jnp.mean(v, -1, keepdims=True)
        c = v - mean
        return c * lax.rsqrt(jnp.mean(c * c, -1, keepdims=True) + NORM_EPSILON) * gain + bias

    xg[tp] = norm(yb[...], g1_ref[...], b1_ref[...]).astype(bf16)
    for i in range(1, NX):
        t = lax.rem(x + i, NX) * 2 + core
        rc(xg.at[tp], xg.at[tp], x_s, x_r.at[tp], {"tp": t}).start()
    rc(xg.at[tp], xg.at[tp], xp_s, x_r.at[TP], partner).start()
    late = list(range(SM + 1, HALF))
    for s in range(mid_a + 1, HALF):
        step_wa(s)
        if late:
            pair(late.pop(0), relay)
    for i in range(1, NX):
        t = lax.rem(x + i, NX) * 2 + core
        got(xg.at[t], x_r.at[t])
        rc(xg.at[t], xg.at[t], xp_s, x_r.at[TP], partner).start()

    for s in late:
        pair(s, relay)
    relay(far)
    for k in range(2):
        got(wa_at(far, k), wa_r.at[far, k])
    got(xg.at[pl.ds(0, NX)], x_r.at[TP])
    got(wb.at[pl.ds(0, NZ), :, pl.ds(FA, FW - FA)], yh_r)

    @pl.loop(0, FW // CW)
    def _(n):
        cols = pl.ds(pl.multiple_of(n * CW, CW), CW)
        up = dot(xg[...].reshape(tok, D), wb[:, :piece, cols].reshape(D, CW))
        hid[:, cols] = jnp.square(jnp.maximum(up, 0.0)).astype(bf16)

    QW = part.shape[3]
    quarters = D // QW
    nb = min(256, QW)
    per = nb // piece

    def down(h):
        @pl.loop(0, QW // nb)
        def _(n):
            w = wb[pl.ds((h * (QW // nb) + n) * per, per), piece:, :].reshape(nb, FW)
            ffn = dot(hid[...], w, NT).astype(bf16)
            part[h, :, :, pl.ds(pl.multiple_of(n * nb, nb), nb)] = ffn.reshape(TP, own_rows, nb)

        for i in range(1, NX + 1):
            t = lax.rem(x + i, NX)
            rc(part.at[h, t * 2 + 1 - core], prb.at[h, t], p_s, p_r.at[h], partner).start()

    def fold(h):
        got(prb.at[h], p_r.at[h])
        for i in range(1, NX):
            t = lax.rem(x + i, NX)
            comb[h, t] = (part[h, t * 2 + core].astype(f32) + prb[h, t].astype(f32)).astype(bf16)
            rc(comb.at[h, t], rr.at[h, x], r_s, r_r.at[h], {"tp": t * 2 + core}).start()

    for h in range(quarters):
        down(h)
        if h > 0:
            fold(h - 1)
    fold(quarters - 1)
    for h in range(quarters):
        cols = slice(h * QW, (h + 1) * QW)
        total = part[h, tp].astype(f32) + prb[h, x].astype(f32) + ALPHA * xg[tp, :, cols].astype(f32)
        if NX > 1:
            got(rr.at[h, pl.ds(0, NX - 1)], r_r.at[h])
            for i in range(1, NX):
                total += rr[h, lax.rem(x + i, NX)].astype(f32)
        yb[:, cols] = total
    last = norm(yb[...], g2_ref[...], b2_ref[...]).astype(bf16)
    wide = D // TP
    for t in range(TP):
        enc[t] = last[:, t * wide : (t + 1) * wide]
    mine = pl.ds(tp * own_rows, own_rows)
    for i in range(1, TP):
        t = lax.rem(tp + i, TP)
        rc(enc.at[t], out_ref.at[mine, :], e_s, e_r, {"tp": t}).start()
    out_ref[mine, :] = enc[tp]

    sent(qb.at[pl.ds(0, NY - 1)], q_s)
    sent(wb.at[pl.ds(0, NY - 1), :, pl.ds(0, FA)], ya_s)
    sent(kvb.at[pl.ds(0, NZ - 1)], kv_s)
    sent(wb.at[pl.ds(0, (NZ - 1) * NY), :, pl.ds(0, FA)], wa_s)
    sent(wb.at[pl.ds(0, NZ - 1), :, pl.ds(FA, FW - FA)], wz_s)
    sent(wb.at[pl.ds(0, 3 * NZ), :, pl.ds(FA, FW - FA)], yf_s)
    sent(oms.at[pl.ds(0, NY * TP - 1)], o_s)
    sent(wo.at[pl.ds(0, NX)], wp_s)
    sent(xg.at[pl.ds(0, NX)], xp_s)
    sent(prb, p_s)
    if NX > 1:
        sent(wo.at[pl.ds(0, NX - 1)], wo_s)
        sent(xg.at[pl.ds(0, NX - 1)], x_s)
        sent(rr.at[:, pl.ds(0, NX - 1)], r_s)
    sent(enc.at[pl.ds(0, TP - 1)], e_s)
    got(out_ref.at[pl.ds(0, (TP - 1) * own_rows), :], e_r)


def solution(mesh):
    SP, TP = mesh.shape["sp"], mesh.shape["tp"]
    NZ, NX = SP // NY, TP // 2

    def local(queries, keys, values, q_gain, key_norm_gain, out_weight, residual, ln1_gain, ln1_bias, up_weight, down_weight, ln2_gain, ln2_bias):
        tok, D, FW = queries.shape[0], out_weight.shape[1], up_weight.shape[1]
        own = tok // TP
        FA = (FW // 128 * 3 // 8) * 128
        piece = up_weight.shape[0]
        rows, cols = rotary_tables(tok * SP, SP)
        quarters = 4
        vm, hbm = pl.BlockSpec(memory_space=pltpu.VMEM), pl.BlockSpec(memory_space=pl.ANY)
        dma = pltpu.SemaphoreType.DMA
        one = dma(())
        V = pltpu.VMEM
        flops = 2 * tok * tok * SP * 256 + 4 * tok * D * FW
        rs = (quarters, NX, own, D // quarters)
        return pl.pallas_call(
            functools.partial(kernel, NZ, NX, FA),
            out_shape=jax.ShapeDtypeStruct((tok, D // TP), bf16),
            in_specs=[vm, vm, vm, vm, vm, hbm, vm, hbm, hbm, hbm, hbm, vm, vm, vm, vm],
            out_specs=vm,
            scratch_shapes=[
                V(rows.shape[1:], f32), V((NY, tok, 128), bf16), V((NZ, tok, 128), bf16), V((NY * tok * 2, 128), bf16),
                V((NY * tok * 2, 128), f32), V((NY * tok * 2, 128), f32),
                V((SP, 2 * piece, FW), bf16), V((TP, 128, D), bf16),
                V((NY * TP, 2 * own, 128), bf16), V((NY * TP, 2 * own, 128), bf16), V((own, TP * 128), bf16),
                V((own, D), f32), V((own, D), bf16), V((TP, own, D), bf16), V((tok, FW), bf16),
                V((quarters, TP, own, D // quarters), bf16), V(rs, bf16), V(rs, bf16), V(rs, bf16), V((TP, own, D // TP), bf16),
                one, dma((NY,)), one, dma((NZ,)), one, dma((NZ, 2)), one, dma((NZ,)),
                one, dma((NY,)), one, dma((NZ, 2)), one, one, dma((2,)), one,
                one, one, one, dma((TP + 1,)), one,
                one, dma((quarters,)), one, dma((quarters,)), one, one, dma((5,)),
            ],
            compiler_params=pltpu.CompilerParams(collective_id=0, has_side_effects=True, vmem_limit_bytes=60000000),
            cost_estimate=pl.CostEstimate(flops=flops, bytes_accessed=30000000, transcendentals=0),
        )(
            queries, keys.T, values.T, q_gain[None], key_norm_gain[None], jnp.asarray(rows), jnp.asarray(cols),
            up_weight, down_weight.T, out_weight, residual, ln1_gain[None], ln1_bias[None], ln2_gain[None], ln2_bias[None],
        )

    return jax.shard_map(
        local,
        mesh=mesh,
        in_specs=(
            P("sp", "tp"), P("sp", "tp"), P("sp", "tp"), P(), P(), P("tp", None), P("sp", None),
            P(), P(), P("sp", "tp"), P("tp", "sp"), P(), P(),
        ),
        out_specs=P("sp", "tp"),
        check_vma=False,
    )
```

time: 138 us -> 104 us (0.75)
  Pallas kernels: 130 us -> 103 us
  local copies, waits for them, and re-layouts: 5.65 us -> 1.57 us
  other arithmetic: 2.04 us -> 0 us
    pallas_call x1, Pallas kernels: 130 us -> 103 us  [local(): pl.pallas_call(functools.partial(kernel, NZ, NX, FA), out_shape=jax.Shape...]
where the time goes in v2:
time: 104 us
  Pallas kernels  103 us (99%)
  local copies, waits for them, and re-layouts  1.57 us (2%)
    pallas_call x1, Pallas kernels, local(): pl.pallas_call(functools.partial(kernel, NZ, NX, FA), out_shape=jax.Shape...  103 us

profile of v2, /device:TPU:1, one launch (start us, length us, event | category | flops | bytes accessed | tf_op | source)
XLA Modules:
  0.0 104.3 jit_solution(3374404021389103956)
XLA Ops:
  0.0 102.7 %shard_map.145 = bf16[256,256]{1,0:T(8,128)(2,1)} custom-call(bf16[256,128]{1,0:T(8,128)(2,1)} %q_ref.1, bf16[64,256]{1,0:T(8,128)(2,1)} %bitcast.10, bf16[64,256]{1,0:T(8,128)(2,1)} %bitcast.11, f32[1,64]{1,0:T(1,128)} %bitcast.16, f32[1,64]{1,0:T(1,128)} %bitcast.17, f32[64,8,384]{2,1,0:T(8,128)} %constant.4.clone.row_ref, ...), custom_call_target="tpu_custom_call" | custom-call | flops 4294967296 | bytes 30000000 | tf_op jit(solution)/shard_map/pallas_call | solution.py:468
  102.7 1.6 %copy.17 = bf16[256,256]{1,0:T(8,128)(2,1)} copy(bf16[256,256]{1,0:T(8,128)(2,1)} %shard_map.145) | data formatting | bytes 262144

commit v3 on v2

--- a/solution.py
+++ b/solution.py
@@ -41,10 +41,10 @@
 
 
 def kernel(
-    NZ, NX, FA,
-    q_ref, k_ref, v_ref, gq_ref, gk_ref, row_ref, col_ref, up_ref, down_ref, wo_own, res_ref, g1_ref, b1_ref, g2_ref, b2_ref,
+    NZ, NX, FU, FD,
+    q_hbm, k_hbm, v_hbm, gq_hbm, gk_hbm, row_ref, col_hbm, up_ref, down_ref, wo_own, res_ref, g1_ref, b1_ref, g2_ref, b2_ref,
     out_ref,
-    rowv, qb, kvb, qx, acc, mx, wb, wo, oms, omr, att, yb, res, xg, hid, part, prb, comb, rr, enc,
+    q_ref, kv_ref, gq_ref, gk_ref, col_ref, ln, rowv, qb, kvb, qx, acc, mx, wb, wo, oms, omr, att, yb, res, xg, hid, part, prb, comb, rr, enc,
     q_s, q_r, kv_s, kv_r, wa_s, wa_r, wz_s, wz_r, ya_s, ya_r, yf_s, yf_r, yh_r, wo_s, wo_r, wp_s, o_s, o_r, x_s, x_r, xp_s,
     p_s, p_r, r_s, r_r, e_s, e_r, loc,
 ):
@@ -59,7 +59,7 @@
     above, below = {"sp": z * NY + yu}, {"sp": z * NY + yd}
     partner = {"tp": x * 2 + 1 - core}
     me = y * TP + tp
-    tok = q_ref.shape[0]
+    tok = q_hbm.shape[0]
     own_rows = tok // TP
     D = wo.shape[2]
     FW = wb.shape[2]
@@ -75,17 +75,6 @@
 
     def sent(ref, ss):
         rc(ref, ref, ss, ss, right).wait_send()
-
-    barrier = pltpu.get_barrier_semaphore()
-    for dev in (right, left):
-        pl.semaphore_signal(barrier, inc=1, device_id=dev, device_id_type=pl.DeviceIdType.MESH)
-
-    @pl.loop(1, NY * TP)
-    def _(i):
-        d = lax.rem(me + i, NY * TP)
-        pl.semaphore_signal(
-            barrier, inc=1, device_id={"sp": z * NY + d // TP, "tp": lax.rem(d, TP)}, device_id_type=pl.DeviceIdType.MESH
-        )
 
     copies = [
         pltpu.make_async_copy(row_ref.at[sp], rowv, loc.at[0]),
@@ -94,15 +83,38 @@
         pltpu.make_async_copy(wo_own, wo.at[tp], loc.at[3]),
         pltpu.make_async_copy(res_ref.at[pl.ds(tp * own_rows, own_rows), :], res, loc.at[4]),
     ]
-    for c in copies:
+    first = [
+        pltpu.make_async_copy(k_hbm, kv_ref.at[pl.ds(0, HEAD), :], loc.at[5]),
+        pltpu.make_async_copy(v_hbm, kv_ref.at[pl.ds(HEAD, HEAD), :], loc.at[6]),
+        copies[0],
+        pltpu.make_async_copy(col_hbm, col_ref, loc.at[7]),
+        pltpu.make_async_copy(gk_hbm, gk_ref, loc.at[8]),
+    ]
+    second = [
+        pltpu.make_async_copy(q_hbm, q_ref, loc.at[9]),
+        pltpu.make_async_copy(gq_hbm, gq_ref, loc.at[10]),
+    ]
+    third = [pltpu.make_async_copy(r, ln.at[i], loc.at[11 + i]) for i, r in enumerate((g1_ref, b1_ref, g2_ref, b2_ref))]
+    for c in first + second + copies[1:] + third:
         c.start()
+
+    barrier = pltpu.get_barrier_semaphore()
+    for dev in (right, left):
+        pl.semaphore_signal(barrier, inc=1, device_id=dev, device_id_type=pl.DeviceIdType.MESH)
+
+    @pl.loop(1, NY * TP)
+    def _(i):
+        d = lax.rem(me + i, NY * TP)
+        pl.semaphore_signal(
+            barrier, inc=1, device_id={"sp": z * NY + d // TP, "tp": lax.rem(d, TP)}, device_id_type=pl.DeviceIdType.MESH
+        )
 
     lane = lax.broadcasted_iota(jnp.int32, (1, 2 * HEAD), 1)
     low = lane < HEAD
-    kv_all = jnp.transpose(jnp.concatenate([k_ref[...].astype(f32), v_ref[...].astype(f32)], 0))
-    gq = jnp.concatenate([gq_ref[...], gq_ref[...]], 1) * (HEAD**-0.5 * LOG2E)
+    for c in first:
+        c.wait()
+    kv_all = jnp.transpose(kv_ref[...].astype(f32))
     gk = jnp.concatenate([gk_ref[...], gk_ref[...]], 1)
-    copies[0].wait()
 
     def spans():
         for r in range(tok // GRID_W):
@@ -122,23 +134,30 @@
 
     pl.semaphore_wait(barrier, NY * TP + 1)
 
-    def wa_at(slot, k):
-        return wb.at[pl.ds(slot * NY + k * (NY // 2), NY // 2), :, pl.ds(0, FA)]
-
-    def wz_at(slot, row):
-        return wb.at[slot * NY + row, :, pl.ds(FA, FW - FA)]
-
-    def half_at(slot, row, k):
-        return wb.at[slot * NY + row, pl.ds(k * piece, piece), pl.ds(FA, FW - FA)]
+    cut = (FU, FD)
+
+    def first_at(row, h):
+        return wb.at[row, pl.ds(h * piece, piece), pl.ds(0, cut[h])]
+
+    def half_at(slot, row, h):
+        return wb.at[slot * NY + row, pl.ds(h * piece, piece), pl.ds(cut[h], FW - cut[h])]
+
+    def amount(rows):
+        return wb.at[pl.ds(0, rows), pl.ds(0, piece), pl.ds(0, FU + FD)]
+
+    def halves(rows, h):
+        return wb.at[pl.ds(0, rows), pl.ds(h * piece, piece), pl.ds(cut[h], FW - cut[h])]
 
     def send_kv(slot, dev):
         rc(kvb.at[slot], kvb.at[slot], kv_s, kv_r.at[slot], dev).start()
 
     def send_wa(slot, dev, k):
-        rc(wa_at(slot, k), wa_at(slot, k), wa_s, wa_r.at[slot, k], dev).start()
-
-    def send_wz(slot, dev):
-        rc(wz_at(slot, y), wz_at(slot, y), wz_s, wz_r.at[slot], dev).start()
+        for h in range(2):
+            r = first_at(slot * NY + k, h)
+            rc(r, r, wa_s, wa_r.at[slot, k], dev).start()
+
+    def send_wz(slot, dev, h):
+        rc(half_at(slot, y, h), half_at(slot, y, h), wz_s.at[h], wz_r.at[slot, h], dev).start()
 
     def minus(s):
         return lax.rem(z + NZ - s, NZ)
@@ -176,35 +195,39 @@
 
         both(s, lambda i: kvb.at[i], kv_r, send_kv, part_of(0), part_of(tok // 2))
 
+    def nothing(i, dev):
+        pass
+
     def step_wz(s):
-        def part_of(k):
-            def f(i, dev):
-                rc(half_at(i, y, k), half_at(i, y, k), wz_s, wz_r.at[i], dev).start()
-
-            return f
-
-        both(s, lambda i: wz_at(i, y), wz_r, send_wz, part_of(0), part_of(1))
+        for h in range(2):
+
+            def go(i, dev, h=h):
+                send_wz(i, dev, h)
+
+            both(s, lambda i, h=h: half_at(i, y, h), wz_r.at[:, h], go, nothing if h else go, go if h else nothing)
+
+    def sub_wa(s, k):
+        def go(i, dev):
+            send_wa(i, dev, k)
+
+        low_half = isinstance(k, int) and k < NY // 2
+        both(s, lambda i: amount(1), wa_r.at[:, k], go, go if low_half else nothing, nothing if low_half else go)
 
     def step_wa(s):
-        for k in range(2):
-
-            def nothing(i, dev):
-                pass
-
-            def go(i, dev, k=k):
-                send_wa(i, dev, k)
-
-            both(s, lambda i, k=k: wa_at(i, k), wa_r.at[:, k], go, go if k == 0 else nothing, go if k == 1 else nothing)
+        for k in range(NY):
+            sub_wa(s, k)
 
     def spread(slot):
-        rc(wz_at(slot, y), wz_at(slot, y), yf_s, yf_r.at[slot, 0], above).start()
-        rc(wz_at(slot, y), wz_at(slot, y), yf_s, yf_r.at[slot, 1], below).start()
+        for h, onward, last in ((0, above, below), (1, below, above)):
+            r = half_at(slot, y, h)
+            rc(r, r, yf_s.at[h], yf_r.at[slot, h], onward).start()
+            rc(r, r, yf_s.at[h], yh_r.at[h], last).start()
 
     def relay(slot):
-        got(wz_at(slot, yd), yf_r.at[slot, 0])
-        rc(half_at(slot, yd, 0), half_at(slot, yd, 0), yf_s, yh_r, above).start()
-        got(wz_at(slot, yu), yf_r.at[slot, 1])
-        rc(half_at(slot, yu, 1), half_at(slot, yu, 1), yf_s, yh_r, below).start()
+        for h, source, onward in ((0, yd, above), (1, yu, below)):
+            r = half_at(slot, source, h)
+            got(r, yf_r.at[slot, h])
+            rc(r, r, yf_s.at[h], yh_r.at[h], onward).start()
 
     def pair(s, f):
         f(minus(s))
@@ -216,10 +239,15 @@
     copies[2].wait()
     for i in range(1, NY):
         t = lax.rem(y + i, NY)
-        own = wb.at[sp, :, pl.ds(0, FA)]
-        rc(own, own, ya_s, ya_r.at[y], {"sp": z * NY + t}).start()
-    send_wz(z, right)
-    send_wz(z, left)
+        for h in range(2):
+            own = first_at(sp, h)
+            rc(own, own, ya_s, ya_r.at[y], {"sp": z * NY + t}).start()
+    for h in range(2):
+        send_wz(z, right, h)
+        send_wz(z, left, h)
+    for c in second:
+        c.wait()
+    gq = jnp.concatenate([gq_ref[...], gq_ref[...]], 1) * (HEAD**-0.5 * LOG2E)
     for span, cs, kv in spans():
         qb[y, span, :] = turn(q_ref[span, :].astype(f32), gq, cs).astype(bf16)
     for i in range(1, NY):
@@ -257,7 +285,7 @@
     acc[...] = jnp.zeros_like(acc)
     mx[...] = jnp.full_like(mx, -1e30)
     spread_q(y)
-    NA = (HALF - 1) // 3
+    beside = HALF - 2
     SM = HALF - 3
 
     @pl.loop(1, HALF)
@@ -269,8 +297,8 @@
         def _():
             for i in range(1, NY):
                 t = lax.rem(y + i, NY)
-                got(wb.at[z * NY + t, :, pl.ds(0, FA)], ya_r.at[t])
-            for k in range(2):
+                got(amount(1), ya_r.at[t])
+            for k in range(NY):
                 send_wa(z, right, k)
                 send_wa(z, left, k)
             for i in range(1, NY):
@@ -279,9 +307,9 @@
                 spread_q(t)
             flash([z])
 
-        @pl.when(lax.rem(s, 3) == 0)
+        @pl.when(s > 1)
         def _():
-            step_wa(s // 3)
+            sub_wa((s - 2) // NY + 1, lax.rem(s - 2, NY))
 
         @pl.when(s <= SM)
         def _():
@@ -289,24 +317,32 @@
 
         flash([minus(s), plus(s)])
 
-        @pl.when(s <= SM + 1)
+        @pl.when((s >= 2) & (s <= SM + 2))
         def _():
-            relay(minus(s - 1))
-
-            @pl.when(s > 1)
+            relay(minus(s - 2))
+
+            @pl.when(s > 2)
             def _():
-                relay(plus(s - 1))
+                relay(plus(s - 2))
 
     far = lax.rem(z + HALF, NZ)
+    for i in range(beside, -(-beside // NY) * NY):
+        sub_wa(i // NY + 1, i % NY)
+    rest = list(range(-(-beside // NY) + 1, HALF))
     got(kvb.at[far], kv_r.at[far])
     flash([far])
 
-    total = pltpu.roll(acc[...], HEAD, 1)
-    lse = mx[...] + jnp.log2(acc[...])
+    o = (acc[...] / pltpu.roll(acc[...], HEAD, 1)).reshape(NY * TP, 2, own_rows, 128)
+    heads = jnp.where(low, pltpu.roll(o[:, 0].reshape(-1, 128), HEAD, 1), o[:, 1].reshape(-1, 128))
+    oms[:, :own_rows, :] = heads.astype(bf16).reshape(NY * TP, own_rows, 128)
+    lse = (mx[...] + jnp.log2(acc[...])).reshape(NY * TP, 2 * own_rows, 128)
+    at = lax.broadcasted_iota(jnp.int32, lse.shape, 1) == lax.broadcasted_iota(jnp.int32, lse.shape, 2)
+    lse = jnp.sum(jnp.where(at, lse, 0.0), 1, keepdims=True)
     hi = lse.astype(bf16).astype(f32)
     mid = (lse - hi).astype(bf16).astype(f32)
-    sumparts = jnp.where(lane < 16, hi, jnp.where(lane < 32, mid, jnp.where(lane < 48, lse - hi - mid, 0.0)))
-    oms[...] = jnp.where(low, sumparts, acc[...] / total).astype(bf16).reshape(oms.shape)
+    row = lax.broadcasted_iota(jnp.int32, (NY * TP, 16, 128), 1)
+    parts = jnp.where(row == 0, hi, jnp.where(row == 1, mid, jnp.where(row == 2, lse - hi - mid, 0.0)))
+    oms[:, own_rows:, :] = parts.astype(bf16)
 
     @pl.loop(1, NY * TP)
     def _(i):
@@ -314,35 +350,42 @@
         rc(oms.at[d], omr.at[me], o_s, o_r, {"sp": z * NY + d // TP, "tp": lax.rem(d, TP)}).start()
 
     omr[me] = oms[me]
-    for s in range(SM + 1, HALF):
+    for s in rest[:1]:
+        step_wa(s)
+    for s in range(SM + 1, HALF - 1):
         pair(s, spread)
-    step_wa(NA + 1)
     if NX > 1:
         got(wo.at[pl.ds(0, NX - 1)], wo_r.at[0])
     for i in range(NX):
         t = lax.rem(x + i, NX) * 2 + core
         rc(wo.at[t], wo.at[t], wp_s, wo_r.at[1], partner).start()
-    got(wz_at(far, y), wz_r.at[far])
-    spread(far)
-    mid_a = min(NA + 3, HALF - 1)
-    for s in range(NA + 2, mid_a + 1):
+    for h in range(2):
+        got(half_at(far, y, h), wz_r.at[far, h])
+    for s in rest[1:2]:
         step_wa(s)
+    pair(HALF - 1, spread)
     got(omr.at[pl.ds(0, NY * TP - 1)], o_r)
 
     @pl.loop(0, TP)
     def _(t):
         msgs = [omr[r * TP + t].astype(f32) for r in range(NY)]
-        lses = [jnp.sum(jnp.where(lane < 48, m, 0.0), -1, keepdims=True) * (1.0 / 16.0) for m in msgs]
+        row = lax.broadcasted_iota(jnp.int32, (own_rows, 128), 0)
+        lses = []
+        for m in msgs:
+            line = jnp.sum(m[own_rows:], 0, keepdims=True)
+            h0, h1 = (jnp.sum(jnp.where(row + at == lane, line, 0.0), -1, keepdims=True) for at in (0, own_rows))
+            lses.append(jnp.where(low, h0, h1))
         top = functools.reduce(jnp.maximum, lses)
         ws = [jnp.exp2(v - top) for v in lses]
-        o = functools.reduce(jnp.add, [w * m for w, m in zip(ws, msgs)]) / functools.reduce(jnp.add, ws)
-        heads = jnp.where(low, pltpu.roll(o[:own_rows], HEAD, 1), o[own_rows:])
-        att[:, pl.ds(pl.multiple_of(t * 128, 128), 128)] = heads.astype(bf16)
+        o = functools.reduce(jnp.add, [w * m[:own_rows] for w, m in zip(ws, msgs)]) / functools.reduce(jnp.add, ws)
+        att[:, pl.ds(pl.multiple_of(t * 128, 128), 128)] = o.astype(bf16)
 
     got(wo.at[pl.ds(0, NX)], wo_r.at[1])
     copies[4].wait()
-
-    CW = 256
+    for c in third:
+        c.wait()
+
+    CW = min(1024, D)
 
     @pl.loop(0, D // CW)
     def _(n):
@@ -355,47 +398,43 @@
         c = v - mean
         return c * lax.rsqrt(jnp.mean(c * c, -1, keepdims=True) + NORM_EPSILON) * gain + bias
 
-    xg[tp] = norm(yb[...], g1_ref[...], b1_ref[...]).astype(bf16)
+    xg[tp] = norm(yb[...], ln[0], ln[1]).astype(bf16)
     for i in range(1, NX):
         t = lax.rem(x + i, NX) * 2 + core
         rc(xg.at[tp], xg.at[tp], x_s, x_r.at[tp], {"tp": t}).start()
     rc(xg.at[tp], xg.at[tp], xp_s, x_r.at[TP], partner).start()
     late = list(range(SM + 1, HALF))
-    for s in range(mid_a + 1, HALF):
+    for s in rest[2:]:
         step_wa(s)
-        if late:
+        if s == rest[2]:
+            spread(far)
+        if late and s < HALF - 1:
             pair(late.pop(0), relay)
+    if not rest[2:]:
+        spread(far)
+    for s in late:
+        pair(s, relay)
+    relay(far)
     for i in range(1, NX):
         t = lax.rem(x + i, NX) * 2 + core
         got(xg.at[t], x_r.at[t])
         rc(xg.at[t], xg.at[t], xp_s, x_r.at[TP], partner).start()
-
-    for s in late:
-        pair(s, relay)
-    relay(far)
-    for k in range(2):
-        got(wa_at(far, k), wa_r.at[far, k])
+    for k in range(NY):
+        got(amount(1), wa_r.at[far, k])
     got(xg.at[pl.ds(0, NX)], x_r.at[TP])
-    got(wb.at[pl.ds(0, NZ), :, pl.ds(FA, FW - FA)], yh_r)
-
-    @pl.loop(0, FW // CW)
-    def _(n):
-        cols = pl.ds(pl.multiple_of(n * CW, CW), CW)
-        up = dot(xg[...].reshape(tok, D), wb[:, :piece, cols].reshape(D, CW))
-        hid[:, cols] = jnp.square(jnp.maximum(up, 0.0)).astype(bf16)
+    for h in range(2):
+        got(halves(2 * NZ, h), yh_r.at[h])
+
+    up = dot(xg[...].reshape(tok, D), wb[:, :piece, :].reshape(D, FW))
+    hid[...] = jnp.square(jnp.maximum(up, 0.0)).astype(bf16)
 
     QW = part.shape[3]
     quarters = D // QW
-    nb = min(256, QW)
-    per = nb // piece
+    per = QW // piece
 
     def down(h):
-        @pl.loop(0, QW // nb)
-        def _(n):
-            w = wb[pl.ds((h * (QW // nb) + n) * per, per), piece:, :].reshape(nb, FW)
-            ffn = dot(hid[...], w, NT).astype(bf16)
-            part[h, :, :, pl.ds(pl.multiple_of(n * nb, nb), nb)] = ffn.reshape(TP, own_rows, nb)
-
+        w = wb[pl.ds(h * per, per), piece:, :].reshape(QW, FW)
+        part[h] = dot(hid[...], w, NT).astype(bf16).reshape(TP, own_rows, QW)
         for i in range(1, NX + 1):
             t = lax.rem(x + i, NX)
             rc(part.at[h, t * 2 + 1 - core], prb.at[h, t], p_s, p_r.at[h], partner).start()
@@ -420,7 +459,7 @@
             for i in range(1, NX):
                 total += rr[h, lax.rem(x + i, NX)].astype(f32)
         yb[:, cols] = total
-    last = norm(yb[...], g2_ref[...], b2_ref[...]).astype(bf16)
+    last = norm(yb[...], ln[2], ln[3]).astype(bf16)
     wide = D // TP
     for t in range(TP):
         enc[t] = last[:, t * wide : (t + 1) * wide]
@@ -428,14 +467,16 @@
     for i in range(1, TP):
         t = lax.rem(tp + i, TP)
         rc(enc.at[t], out_ref.at[mine, :], e_s, e_r, {"tp": t}).start()
-    out_ref[mine, :] = enc[tp]
+    out_copy = pltpu.make_async_copy(enc.at[tp], out_ref.at[mine, :], loc.at[15])
+    out_copy.start()
 
     sent(qb.at[pl.ds(0, NY - 1)], q_s)
-    sent(wb.at[pl.ds(0, NY - 1), :, pl.ds(0, FA)], ya_s)
+    sent(amount(NY - 1), ya_s)
     sent(kvb.at[pl.ds(0, NZ - 1)], kv_s)
-    sent(wb.at[pl.ds(0, (NZ - 1) * NY), :, pl.ds(0, FA)], wa_s)
-    sent(wb.at[pl.ds(0, NZ - 1), :, pl.ds(FA, FW - FA)], wz_s)
-    sent(wb.at[pl.ds(0, 3 * NZ), :, pl.ds(FA, FW - FA)], yf_s)
+    sent(amount((NZ - 1) * NY), wa_s)
+    for h in range(2):
+        sent(halves(NZ - 1, h), wz_s.at[h])
+        sent(halves(3 * NZ, h), yf_s.at[h])
     sent(oms.at[pl.ds(0, NY * TP - 1)], o_s)
     sent(wo.at[pl.ds(0, NX)], wp_s)
     sent(xg.at[pl.ds(0, NX)], xp_s)
@@ -445,6 +486,7 @@
         sent(xg.at[pl.ds(0, NX - 1)], x_s)
         sent(rr.at[:, pl.ds(0, NX - 1)], r_s)
     sent(enc.at[pl.ds(0, TP - 1)], e_s)
+    out_copy.wait()
     got(out_ref.at[pl.ds(0, (TP - 1) * own_rows), :], e_r)
 
 
@@ -455,32 +497,33 @@
     def local(queries, keys, values, q_gain, key_norm_gain, out_weight, residual, ln1_gain, ln1_bias, up_weight, down_weight, ln2_gain, ln2_bias):
         tok, D, FW = queries.shape[0], out_weight.shape[1], up_weight.shape[1]
         own = tok // TP
-        FA = (FW // 128 * 3 // 8) * 128
+        FU, FD = FW // 1024 * 384, FW // 1024 * 384
         piece = up_weight.shape[0]
         rows, cols = rotary_tables(tok * SP, SP)
         quarters = 4
-        vm, hbm = pl.BlockSpec(memory_space=pltpu.VMEM), pl.BlockSpec(memory_space=pl.ANY)
+        hbm = pl.BlockSpec(memory_space=pl.ANY)
         dma = pltpu.SemaphoreType.DMA
         one = dma(())
         V = pltpu.VMEM
         flops = 2 * tok * tok * SP * 256 + 4 * tok * D * FW
         rs = (quarters, NX, own, D // quarters)
         return pl.pallas_call(
-            functools.partial(kernel, NZ, NX, FA),
+            functools.partial(kernel, NZ, NX, FU, FD),
             out_shape=jax.ShapeDtypeStruct((tok, D // TP), bf16),
-            in_specs=[vm, vm, vm, vm, vm, hbm, vm, hbm, hbm, hbm, hbm, vm, vm, vm, vm],
-            out_specs=vm,
+            in_specs=[hbm] * 15,
+            out_specs=hbm,
             scratch_shapes=[
+                V((tok, 128), bf16), V((2 * HEAD, tok), bf16), V((1, HEAD), f32), V((1, HEAD), f32), V(cols.shape, f32), V((4, 1, D), f32),
                 V(rows.shape[1:], f32), V((NY, tok, 128), bf16), V((NZ, tok, 128), bf16), V((NY * tok * 2, 128), bf16),
                 V((NY * tok * 2, 128), f32), V((NY * tok * 2, 128), f32),
                 V((SP, 2 * piece, FW), bf16), V((TP, 128, D), bf16),
-                V((NY * TP, 2 * own, 128), bf16), V((NY * TP, 2 * own, 128), bf16), V((own, TP * 128), bf16),
+                V((NY * TP, own + 16, 128), bf16), V((NY * TP, own + 16, 128), bf16), V((own, TP * 128), bf16),
                 V((own, D), f32), V((own, D), bf16), V((TP, own, D), bf16), V((tok, FW), bf16),
                 V((quarters, TP, own, D // quarters), bf16), V(rs, bf16), V(rs, bf16), V(rs, bf16), V((TP, own, D // TP), bf16),
-                one, dma((NY,)), one, dma((NZ,)), one, dma((NZ, 2)), one, dma((NZ,)),
-                one, dma((NY,)), one, dma((NZ, 2)), one, one, dma((2,)), one,
+                one, dma((NY,)), one, dma((NZ,)), one, dma((NZ, NY)), dma((2,)), dma((NZ, 2)),
+                one, dma((NY,)), dma((2,)), dma((NZ, 2)), dma((2,)), one, dma((2,)), one,
                 one, one, one, dma((TP + 1,)), one,
-                one, dma((quarters,)), one, dma((quarters,)), one, one, dma((5,)),
+                one, dma((quarters,)), one, dma((quarters,)), one, one, dma((16,)),
             ],
             compiler_params=pltpu.CompilerParams(collective_id=0, has_side_effects=True, vmem_limit_bytes=60000000),
             cost_estimate=pl.CostEstimate(flops=flops, bytes_accessed=30000000, transcendentals=0),

time: 104 us -> 97.4 us (0.937)
  Pallas kernels: 103 us -> 95.7 us
    pallas_call x1, Pallas kernels: 103 us -> 95.7 us  [local(): pl.pallas_call(functools.partial(kernel, NZ, NX, FU, FD), out_shape=jax.S...]
where the time goes in v3:
time: 97.4 us; the launch traced here: 97.3 us
  Pallas kernels  95.7 us (98%)
  local copies, waits for them, and re-layouts  1.57 us (2%)
    pallas_call x1, Pallas kernels, local(): pl.pallas_call(functools.partial(kernel, NZ, NX, FU, FD), out_shape=jax.S...  95.7 us

profile of v3, /device:TPU:1, one launch (start us, length us, event | category | flops | bytes accessed | tf_op | source)
XLA Modules:
  0.0 97.3 jit_solution(1186063618977448068)
XLA Ops:
  0.0 95.7 %shard_map.145 = bf16[256,256]{1,0:T(8,128)(2,1)} custom-call(bf16[256,128]{1,0:T(8,128)(2,1)} %q_hbm.1, bf16[64,256]{1,0:T(8,128)(2,1)} %bitcast.10, bf16[64,256]{1,0:T(8,128)(2,1)} %bitcast.11, f32[1,64]{1,0:T(1,128)} %bitcast.16, f32[1,64]{1,0:T(1,128)} %bitcast.17, f32[64,8,384]{2,1,0:T(8,128)} %constant.4.clone.row_ref, ...), custom_call_target="tpu_custom_call" | custom-call | flops 4294967296 | bytes 30000000 | tf_op jit(solution)/shard_map/pallas_call | solution.py:510
  95.7 1.6 %copy.17 = bf16[256,256]{1,0:T(8,128)(2,1)} copy(bf16[256,256]{1,0:T(8,128)(2,1)} %shard_map.145) | data formatting | bytes 262144

commit v4 on v3

--- a/solution.py
+++ b/solution.py
@@ -207,11 +207,13 @@
             both(s, lambda i, h=h: half_at(i, y, h), wz_r.at[:, h], go, nothing if h else go, go if h else nothing)
 
     def sub_wa(s, k):
-        def go(i, dev):
-            send_wa(i, dev, k)
-
-        low_half = isinstance(k, int) and k < NY // 2
-        both(s, lambda i: amount(1), wa_r.at[:, k], go, go if low_half else nothing, nothing if low_half else go)
+        other = (k + NY // 2) % NY if isinstance(k, int) else lax.rem(k + NY // 2, NY)
+        got(amount(1), wa_r.at[minus(s), k])
+        if not isinstance(s, int) or s < HALF - 1 or k < NY // 2:
+            send_wa(minus(s), right, k)
+        got(amount(1), wa_r.at[plus(s), other])
+        if not isinstance(s, int) or s < HALF - 1 or k < NY // 2:
+            send_wa(plus(s), left, other)
 
     def step_wa(s):
         for k in range(NY):
@@ -300,7 +302,7 @@
                 got(amount(1), ya_r.at[t])
             for k in range(NY):
                 send_wa(z, right, k)
-                send_wa(z, left, k)
+                send_wa(z, left, (k + NY // 2) % NY)
             for i in range(1, NY):
                 t = lax.rem(y + i, NY)
                 got(qb.at[t], q_r.at[t])
@@ -404,17 +406,25 @@
         rc(xg.at[tp], xg.at[tp], x_s, x_r.at[tp], {"tp": t}).start()
     rc(xg.at[tp], xg.at[tp], xp_s, x_r.at[TP], partner).start()
     late = list(range(SM + 1, HALF))
+    relayed = False
     for s in rest[2:]:
         step_wa(s)
         if s == rest[2]:
             spread(far)
         if late and s < HALF - 1:
             pair(late.pop(0), relay)
+        if s == HALF - 2:
+            for k in late:
+                pair(k, relay)
+            late = []
+            relay(far)
+            relayed = True
     if not rest[2:]:
         spread(far)
     for s in late:
         pair(s, relay)
-    relay(far)
+    if not relayed:
+        relay(far)
     for i in range(1, NX):
         t = lax.rem(x + i, NX) * 2 + core
         got(xg.at[t], x_r.at[t])
@@ -509,9 +519,9 @@
         rs = (quarters, NX, own, D // quarters)
         return pl.pallas_call(
             functools.partial(kernel, NZ, NX, FU, FD),
-            out_shape=jax.ShapeDtypeStruct((tok, D // TP), bf16),
+            out_shape=pltpu.VMEM((tok, D // TP), bf16),
             in_specs=[hbm] * 15,
-            out_specs=hbm,
+            out_specs=pl.BlockSpec(memory_space=pltpu.VMEM),
             scratch_shapes=[
                 V((tok, 128), bf16), V((2 * HEAD, tok), bf16), V((1, HEAD), f32), V((1, HEAD), f32), V(cols.shape, f32), V((4, 1, D), f32),
                 V(rows.shape[1:], f32), V((NY, tok, 128), bf16), V((NZ, tok, 128), bf16), V((NY * tok * 2, 128), bf16),

time: 97.4 us -> 94.8 us (0.973)
  Pallas kernels: 95.7 us -> 94 us
    pallas_call x1, Pallas kernels: 95.7 us -> 94 us  [local(): pl.pallas_call(functools.partial(kernel, NZ, NX, FU, FD), out_shape=pltpu...]
where the time goes in v4:
time: 94.8 us; the launch traced here: 94.7 us
  Pallas kernels  94 us (99%)
    pallas_call x1, Pallas kernels, local(): pl.pallas_call(functools.partial(kernel, NZ, NX, FU, FD), out_shape=pltpu...  94 us

profile of v4, /device:TPU:1, one launch (start us, length us, event | category | flops | bytes accessed | tf_op | source)
XLA Modules:
  0.0 94.7 jit_solution(6701267777418916481)
XLA Ops:
  0.0 94.0 %shard_map.145 = bf16[256,256]{1,0:T(8,128)(2,1)S(1)} custom-call(bf16[256,128]{1,0:T(8,128)(2,1)} %q_hbm.1, bf16[64,256]{1,0:T(8,128)(2,1)} %bitcast.10, bf16[64,256]{1,0:T(8,128)(2,1)} %bitcast.11, f32[1,64]{1,0:T(1,128)} %bitcast.16, f32[1,64]{1,0:T(1,128)} %bitcast.17, f32[64,8,384]{2,1,0:T(8,128)} %constant.4.clone.row_ref, ...), custom_call_target="tpu_custom_call" | custom-call | flops 4294967296 | bytes 30000000 | tf_op jit(solution)/shard_map/pallas_call | solution.py:520
  94.0 0.7 copy.17

commit v5 on v4

--- a/solution.py
+++ b/solution.py
@@ -46,7 +46,7 @@
     out_ref,
     q_ref, kv_ref, gq_ref, gk_ref, col_ref, ln, rowv, qb, kvb, qx, acc, mx, wb, wo, oms, omr, att, yb, res, xg, hid, part, prb, comb, rr, enc,
     q_s, q_r, kv_s, kv_r, wa_s, wa_r, wz_s, wz_r, ya_s, ya_r, yf_s, yf_r, yh_r, wo_s, wo_r, wp_s, o_s, o_r, x_s, x_r, xp_s,
-    p_s, p_r, r_s, r_r, e_s, e_r, loc,
+    p_s, p_r, r_s, r_r, e_s, e_r, loc, left_in,
 ):
     TP = 2 * NX
     HALF = NZ // 2
@@ -99,8 +99,7 @@
         c.start()
 
     barrier = pltpu.get_barrier_semaphore()
-    for dev in (right, left):
-        pl.semaphore_signal(barrier, inc=1, device_id=dev, device_id_type=pl.DeviceIdType.MESH)
+    pl.semaphore_signal(barrier, inc=1, device_id=left, device_id_type=pl.DeviceIdType.MESH)
 
     @pl.loop(1, NY * TP)
     def _(i):
@@ -132,7 +131,8 @@
     for span, cs, kv in spans():
         kvb[z, span, :] = jnp.where(low, turn(kv, gk, cs), kv).astype(bf16)
 
-    pl.semaphore_wait(barrier, NY * TP + 1)
+    pl.semaphore_wait(barrier, NY * TP)
+    pl.semaphore_signal(left_in, inc=1, device_id=right, device_id_type=pl.DeviceIdType.MESH)
 
     cut = (FU, FD)
 
@@ -236,7 +236,6 @@
         f(plus(s))
 
     send_kv(z, right)
-    send_kv(z, left)
     copies[1].wait()
     copies[2].wait()
     for i in range(1, NY):
@@ -246,6 +245,9 @@
             rc(own, own, ya_s, ya_r.at[y], {"sp": z * NY + t}).start()
     for h in range(2):
         send_wz(z, right, h)
+    pl.semaphore_wait(left_in, 1)
+    send_kv(z, left)
+    for h in range(2):
         send_wz(z, left, h)
     for c in second:
         c.wait()
@@ -533,7 +535,7 @@
                 one, dma((NY,)), one, dma((NZ,)), one, dma((NZ, NY)), dma((2,)), dma((NZ, 2)),
                 one, dma((NY,)), dma((2,)), dma((NZ, 2)), dma((2,)), one, dma((2,)), one,
                 one, one, one, dma((TP + 1,)), one,
-                one, dma((quarters,)), one, dma((quarters,)), one, one, dma((16,)),
+                one, dma((quarters,)), one, dma((quarters,)), one, one, dma((16,)), pltpu.SemaphoreType.REGULAR,
             ],
             compiler_params=pltpu.CompilerParams(collective_id=0, has_side_effects=True, vmem_limit_bytes=60000000),
             cost_estimate=pl.CostEstimate(flops=flops, bytes_accessed=30000000, transcendentals=0),

time: 94.8 us -> 95.5 us (level)
  no operation moved by 1% of the time
where the time goes in v5:
time: 95.5 us; the launch traced here: 95.3 us
  Pallas kernels  94.7 us (99%)
    pallas_call x1, Pallas kernels, local(): pl.pallas_call(functools.partial(kernel, NZ, NX, FU, FD), out_shape=pltpu...  94.7 us

profile of v5, /device:TPU:1, one launch (start us, length us, event | category | flops | bytes accessed | tf_op | source)
XLA Modules:
  0.0 95.3 jit_solution(4206398593684998879)
XLA Ops:
  0.0 94.7 %shard_map.145 = bf16[256,256]{1,0:T(8,128)(2,1)S(1)} custom-call(bf16[256,128]{1,0:T(8,128)(2,1)} %q_hbm.1, bf16[64,256]{1,0:T(8,128)(2,1)} %bitcast.10, bf16[64,256]{1,0:T(8,128)(2,1)} %bitcast.11, f32[1,64]{1,0:T(1,128)} %bitcast.16, f32[1,64]{1,0:T(1,128)} %bitcast.17, f32[64,8,384]{2,1,0:T(8,128)} %constant.4.clone.row_ref, ...), custom_call_target="tpu_custom_call" | custom-call | flops 4294967296 | bytes 30000000 | tf_op jit(solution)/shard_map/pallas_call | solution.py:522
  94.7 0.7 copy.17
